TPU v7x, 32 devices: a whole 2x2x4 slice. The times are simulated.
32 devices in a mesh: ep: 4 (over y, x), tp: 8 (over z, core).
Axes of the slice: x: 2, y: 2, z: 4, core: 2. Of those that a mesh axis runs over, the one named last changes fastest.
Arguments:
- tokens: bfloat16 [256, 4096], P('ep'), may hold values from -6 to 6
- norm_gain: float32 [4096], replicated, may hold values from 0.1 to 1.9
- ffn_gain: float32 [4096], replicated, may hold values from 0.1 to 1.9
- w_in: bfloat16 [4096, 2048], P(None, 'tp'), may hold values from -0.09375 to 0.09375
- decay_rate: float32 [8192], P('tp'), may hold values from 0.02 to 2
- frequency: float32 [8192], P('tp'), may hold values from -3.140625 to 3.140625
- log_step: float32 [128], P('tp'), may hold values from -2.3 to 0
- input_real: float32 [16, 8192], P(None, 'tp'), may hold values from -1 to 1
- input_imag: float32 [16, 8192], P(None, 'tp'), may hold values from -1 to 1
- readout_real: float32 [16, 8192], P(None, 'tp'), may hold values from -0.5 to 0.5
- readout_imag: float32 [16, 8192], P(None, 'tp'), may hold values from -0.5 to 0.5
- skip_gain: float32 [2048], P('tp'), may hold values from -4 to 4
- state_real: float32 [256, 8192], P('ep', 'tp'), may hold values from -6 to 6
- state_imag: float32 [256, 8192], P('ep', 'tp'), may hold values from -6 to 6
- w_out: bfloat16 [2048, 4096], P('tp'), may hold values from -0.125 to 0.125
- shared_gate: bfloat16 [4096, 1024], P(None, 'tp'), may hold values from -0.09375 to 0.09375
- shared_up: bfloat16 [4096, 1024], P(None, 'tp'), may hold values from -0.09375 to 0.09375
- shared_down: bfloat16 [1024, 4096], P('tp'), may hold values from -0.1875 to 0.1875
- expert_gate: bfloat16 [16, 4096, 1024], P('ep', 'tp'), may hold values from -0.09375 to 0.09375
- expert_up: bfloat16 [16, 4096, 1024], P('ep', 'tp'), may hold values from -0.09375 to 0.09375
- expert_down: bfloat16 [16, 1024, 4096], P('ep', None, 'tp'), may hold values from -0.1875 to 0.1875
- routing: int32 [256, 4], P('ep'), may hold values from 0 to 15, all different within a row; in each aligned block of 64 rows (0 to 63, 64 to 127, ...) at most 32 rows name the same one
- route_weight: float32 [256, 4], P('ep'), may hold values from 0.1 to 1
Outputs:
- mixed: bfloat16 [256, 4096], P('ep', 'tp')
- new_state_real: float32 [256, 8192], P('ep', 'tp')
- new_state_imag: float32 [256, 8192], P('ep', 'tp')
Inputs may be any that keep to these rules, and one draw needn't show every extreme that they name: `routing`: each row names 4 different experts. In the rows of one index of ep (aligned blocks of 64 rows) no expert is named more than 32 times, and in every draw some expert is named exactly 32 times in some block.
All inputs are finite; a program needn't handle non-finite values.
Results may differ from a plain program's by a relative error of at most 0.02.
Values may be sent and summed in bfloat16 or wider, within the bound.
A program may use at most 64 MiB of HBM per device.

v0:
```python
import jax
import jax.numpy as jnp
from jax import lax
from jax.sharding import PartitionSpec as P

EPS = 1e-06
ROUTED_SCALE = 2.5
HIGH = lax.Precision.HIGHEST


def rms_scale(values_in, gains):
    values = values_in.astype(jnp.float32)
    factor = lax.rsqrt(jnp.mean(values * values, axis=-1, keepdims=True) + EPS)
    return (values * factor * gains).astype(jnp.bfloat16)


def state_update(
    normed,
    w_in,
    decay_rate,
    frequency,
    log_step,
    input_real,
    input_imag,
    readout_real,
    readout_imag,
    skip_gain,
    state_real,
    state_imag,
):
    seq_count = normed.shape[0]
    groups = log_step.shape[0]
    chan_count = skip_gain.shape[0] // groups
    state_width = decay_rate.shape[0] // groups
    drive_rows = jnp.dot(normed, w_in, preferred_element_type=jnp.float32).astype(jnp.bfloat16)
    drive_f = drive_rows.astype(jnp.float32).reshape(seq_count, groups, chan_count)
    decays = decay_rate.reshape(groups, state_width)
    omegas = frequency.reshape(groups, state_width)
    step_size = jnp.exp(log_step)[:, None]
    pole_mag = jnp.exp(-decays * step_size)
    pole_angle = omegas * step_size
    pole_re = pole_mag * jnp.cos(pole_angle)
    pole_im = pole_mag * jnp.sin(pole_angle)
    pole_norm = decays * decays + omegas * omegas
    diff_re = pole_re - 1.0
    lift_re = (-decays * diff_re + omegas * pole_im) / pole_norm
    lift_im = (-decays * pole_im - omegas * diff_re) / pole_norm
    in_re = input_real.reshape(chan_count, groups, state_width)
    in_im = input_imag.reshape(chan_count, groups, state_width)
    push_re = jnp.einsum("sgh,hgp->sgp", drive_f, in_re, precision=HIGH)
    push_im = jnp.einsum("sgh,hgp->sgp", drive_f, in_im, precision=HIGH)
    old_re = state_real.reshape(seq_count, groups, state_width)
    old_im = state_imag.reshape(seq_count, groups, state_width)
    new_re = pole_re * old_re - pole_im * old_im + lift_re * push_re - lift_im * push_im
    new_im = pole_re * old_im + pole_im * old_re + lift_re * push_im + lift_im * push_re
    out_re = readout_real.reshape(chan_count, groups, state_width)
    out_im = readout_imag.reshape(chan_count, groups, state_width)
    read_rows = jnp.einsum("sgp,hgp->sgh", new_re, out_re, precision=HIGH) - jnp.einsum(
        "sgp,hgp->sgh", new_im, out_im, precision=HIGH
    )
    read_rows = read_rows + skip_gain.reshape(groups, chan_count) * drive_f
    activated = jax.nn.gelu(read_rows).reshape(seq_count, groups * chan_count).astype(jnp.bfloat16)
    return (
        activated,
        new_re.reshape(seq_count, groups * state_width),
        new_im.reshape(seq_count, groups * state_width),
    )


def local(
    tokens,
    norm_gain,
    ffn_gain,
    w_in,
    decay_rate,
    frequency,
    log_step,
    input_real,
    input_imag,
    readout_real,
    readout_imag,
    skip_gain,
    state_real,
    state_imag,
    w_out,
    shared_gate,
    shared_up,
    shared_down,
    expert_gate,
    expert_up,
    expert_down,
    routing,
    route_weight,
):
    seq_count, model_width = tokens.shape
    tp_count = lax.axis_size("tp")
    ep_count = lax.axis_size("ep")
    slice_width = model_width // tp_count
    offset = lax.axis_index("tp") * slice_width
    normed = rms_scale(tokens, norm_gain)
    activated, new_real, new_imag = state_update(
        normed,
        w_in,
        decay_rate,
        frequency,
        log_step,
        input_real,
        input_imag,
        readout_real,
        readout_imag,
        skip_gain,
        state_real,
        state_imag,
    )
    mixer_terms = jnp.dot(activated, w_out, preferred_element_type=jnp.float32)
    mixer_own = lax.psum_scatter(mixer_terms, "tp", scatter_dimension=1, tiled=True)
    own_tokens = lax.dynamic_slice_in_dim(tokens, offset, slice_width, 1)
    resid_own = (own_tokens.astype(jnp.float32) + mixer_own).astype(jnp.bfloat16)
    resid_f = resid_own.astype(jnp.float32)
    square_sum = lax.psum(jnp.sum(resid_f * resid_f, axis=1, keepdims=True), "tp")
    factor = lax.rsqrt(square_sum / model_width + EPS)
    gain_own = lax.dynamic_slice_in_dim(ffn_gain, offset, slice_width, 0)
    rows_own = (resid_f * factor * gain_own).astype(jnp.bfloat16)
    ffn_rows = lax.all_gather(rows_own, "tp", axis=1, tiled=True)
    expert_dev = expert_gate.shape[0]
    expert_count = expert_dev * ep_count
    top_count = routing.shape[1]
    capacity = 2 * seq_count * top_count // expert_count
    slot_count = expert_count * capacity
    flat_ids = routing.reshape(-1)
    one_hot = (flat_ids[:, None] == jnp.arange(expert_count, dtype=jnp.int32)[None, :]).astype(
        jnp.int32
    )
    earlier = jnp.cumsum(one_hot, axis=0) - one_hot
    slot_rank = jnp.sum(earlier * one_hot, axis=1)
    target = flat_ids * capacity + slot_rank
    slot_ids = jnp.arange(slot_count, dtype=jnp.int32)
    placed = (target[None, :] == slot_ids[:, None]).reshape(slot_count, seq_count, top_count)
    dispatch_map = jnp.sum(placed.astype(jnp.float32), axis=2).astype(jnp.bfloat16)
    outgoing = jnp.dot(dispatch_map, rows_own, preferred_element_type=jnp.float32).astype(
        jnp.bfloat16
    )
    outgoing = outgoing.reshape(ep_count, expert_dev * capacity, slice_width)
    incoming = lax.all_to_all(outgoing, "ep", split_axis=0, concat_axis=0, tiled=True)
    arrived = incoming.reshape(ep_count, expert_dev, capacity, slice_width)
    gate_part = jnp.einsum(
        "secd,edf->secf", arrived, expert_gate, preferred_element_type=jnp.float32
    )
    up_part = jnp.einsum("secd,edf->secf", arrived, expert_up, preferred_element_type=jnp.float32)
    gate_full, up_full = (
        lax.psum(gate_part.astype(jnp.bfloat16), "tp").astype(jnp.float32),
        lax.psum(up_part.astype(jnp.bfloat16), "tp").astype(jnp.float32),
    )
    inner_rows = (jax.nn.silu(gate_full) * up_full).astype(jnp.bfloat16)
    expert_terms = jnp.einsum(
        "secf,efd->secd", inner_rows, expert_down, preferred_element_type=jnp.float32
    )
    returned = lax.all_to_all(
        expert_terms.reshape(ep_count, expert_dev * capacity, slice_width).astype(jnp.bfloat16),
        "ep",
        split_axis=0,
        concat_axis=0,
        tiled=True,
    ).astype(jnp.float32)
    weights = route_weight / jnp.sum(route_weight, axis=1, keepdims=True) * ROUTED_SCALE
    chosen = target.reshape(seq_count, top_count)[:, :, None] == slot_ids[None, None, :]
    combine = jnp.sum(jnp.where(chosen, weights[:, :, None], 0.0), axis=1)
    routed = jnp.dot(combine, returned.reshape(slot_count, slice_width), precision=HIGH)
    shared_gate_rows = jnp.dot(ffn_rows, shared_gate, preferred_element_type=jnp.float32)
    shared_up_rows = jnp.dot(ffn_rows, shared_up, preferred_element_type=jnp.float32)
    shared_inner = (jax.nn.silu(shared_gate_rows) * shared_up_rows).astype(jnp.bfloat16)
    shared_terms = jnp.dot(shared_inner, shared_down, preferred_element_type=jnp.float32)
    shared_own = lax.psum_scatter(
        shared_terms.astype(jnp.bfloat16), "tp", scatter_dimension=1, tiled=True
    ).astype(jnp.float32)
    mixed = (resid_own.astype(jnp.float32) + shared_own + routed).astype(jnp.bfloat16)
    return (mixed, new_real, new_imag)


def solution(mesh):
    placed = (
        P("ep", None),
        P(),
        P(),
        P(None, "tp"),
        P("tp"),
        P("tp"),
        P("tp"),
        P(None, "tp"),
        P(None, "tp"),
        P(None, "tp"),
        P(None, "tp"),
        P("tp"),
        P("ep", "tp"),
        P("ep", "tp"),
        P("tp", None),
        P(None, "tp"),
        P(None, "tp"),
        P("tp", None),
        P("ep", "tp", None),
        P("ep", "tp", None),
        P("ep", None, "tp"),
        P("ep", None),
        P("ep", None),
    )
    return jax.shard_map(
        local,
        mesh=mesh,
        in_specs=placed,
        out_specs=(P("ep", "tp"), P("ep", "tp"), P("ep", "tp")),
        check_vma=False,
    )
```

profile of v0, /device:TPU:0, one launch (start us, length us, event | category | flops | bytes accessed | tf_op | source)
XLA Modules:
  0.0 197.0 jit_solution(18267901409263895610)
XLA Ops:
  7.3 0.8 exp.27
  8.1 1.2 fusion.34
  9.4 0.8 reshape.245
  10.1 0.8 mul.328
  10.9 0.7 fusion.74
  11.7 2.3 %convolution_convert_fusion.2 = bf16[64,256]{1,0:T(8,128)(2,1)S(1)} fusion(bf16[4096,256]{1,0:T(8,128)(2,1)} %param.26, bf16[64,4096]{1,0:T(8,128)(2,1)} %param.23, f32[4096]{0:T(1024)} %param.24, f32[64]{0:T(128)S(1)} %add_rsqrt_fusion), kind=kOutput, calls=%fused_computation.28 | convolution fusion | flops 135282688 | bytes 2670848 | tf_op jit(solution)/shard_map/dot_general | solution.py:35
  14.0 0.1 copy.78
  14.2 0.1 reshape.249
  14.4 0.7 reshape.251
  15.2 1.0 reshape.246
  16.1 0.9 reshape.247
  17.1 0.4 fusion.57
  17.5 0.1 cosine_multiply_fusion
  17.6 1.9 bitcast_add_fusion
  19.6 0.9 fusion.55
  20.5 1.0 fusion.50
  21.5 1.5 fusion.75
  23.1 0.1 copy.85
  23.2 0.1 eq.56
  23.3 0.1 eq.52
  23.5 0.6 reduce-window.6
  24.1 0.2 slice_reduce_fusion
  24.3 0.1 fusion.69
  24.4 0.1 reduce_sum.59
  24.6 0.8 dynamic_slice.7
  25.3 0.1 convert_reduce_fusion
  25.5 33.1 %reduce-scatter.3.cloned.1.call-done = f32[64,512]{1,0:T(8,128)} async-done(((f32[64,4096]{1,0:T(8,128)}), f32[64,512]{1,0:T(8,128)}) %reduce-scatter.3.cloned.1.call-update) | async-done | bytes 131088 | tf_op jit(solution)/shard_map/reduce_scatter | solution.py:116
  58.5 1.0 fusion.51
  59.6 13.9 %psum.21 = f32[64,1]{0,1:T(1,128)S(1)} all-reduce(f32[64,1]{0,1:T(1,128)S(1)} %bitcast.105), channel_id=1, replica_groups=mesh['ep'=4,'tp'=8] {'tp'}, use_global_device_ids=true, to_apply=%region_3.0 | all-reduce | flops 64 | bytes 512 | tf_op jit(solution)/shard_map/psum | solution.py:120
  73.4 0.1 fusion.53
  73.5 0.3 convolution_convert_fusion.1
  73.9 11.7 %all_to_all.10 = bf16[4,128,512]{2,1,0:T(8,128)(2,1)S(1)} all-to-all(bf16[4,128,512]{2,1,0:T(8,128)(2,1)S(1)} %bitcast.99), channel_id=1, replica_groups=mesh['ep'=4,'tp'=8] {'ep'}, dimensions={0} | all-to-all | bytes 1048576 | tf_op jit(solution)/shard_map/all_to_all | solution.py:144
  85.6 4.0 %fusion.17 = bf16[4,4,32,1024]{3,2,0,1:T(8,128)(2,1)} fusion(bf16[4,512,1024]{2,1,0:T(8,128)(2,1)} %param.42, bf16[4,4,32,512]{3,2,1,0:T(8,128)(2,1)S(1)} %bitcast.97), kind=kOutput, calls=%fused_computation.16 | convolution fusion | flops 537395200 | bytes 5767168 | tf_op jit(solution)/shard_map/secd,edf->secf/dot_general | solution.py:149
  89.6 1.7 fusion.20
  91.4 16.5 %all_gather.3 = bf16[64,4096]{1,0:T(8,128)(2,1)S(1)} all-gather(bf16[64,512]{1,0:T(8,128)(2,1)S(1)} %fusion.53), channel_id=1, replica_groups=mesh['ep'=4,'tp'=8] {'tp'}, dimensions={1}, use_global_device_ids=true | all-gather | bytes 589824 | tf_op jit(solution)/shard_map/all_gather | solution.py:124
  107.9 1.5 fusion.76
  109.5 3.0 %convolution_convert_fusion = bf16[64,4096]{1,0:T(8,128)(2,1)} fusion(bf16[128,4096]{1,0:T(8,128)(2,1)} %param.40, bf16[64,4096]{1,0:T(8,128)(2,1)S(1)} %all_gather.3, bf16[4096,128]{1,0:T(8,128)(2,1)} %param.39, f32[64,128]{1,0:T(8,128)S(1)} %fusion.76), kind=kOutput, calls=%fused_computation | convolution fusion | flops 134529024 | bytes 3178496 | tf_op jit(solution)/shard_map/dot_general | solution.py:172
  112.5 42.7 %all-reduce.3.cloned.1.call-done = (bf16[4,4,32,1024]{3,2,0,1:T(8,128)(2,1)}, bf16[4,4,32,1024]{3,2,0,1:T(8,128)(2,1)}) async-done(((bf16[4,4,32,1024]{3,2,0,1:T(8,128)(2,1)}, bf16[4,4,32,1024]{3,2,0,1:T(8,128)(2,1)}), (bf16[4,4,32,1024]{3,2,0,1:T(8,128)(2,1)}, bf16[4,4,32,1024]{3,2,0,1:T(8,128)(2,1)})) %all-reduce.3.cloned.1.call-update) | async-done | bytes 2097168 | tf_op jit(solution)/shard_map/psum | solution.py:152
  155.1 3.7 %fusion.26 = bf16[4,4,32,512]{3,2,0,1:T(8,128)(2,1)S(1)} fusion(bf16[4,1024,512]{2,1,0:T(8,128)(2,1)} %param.43, bf16[4,4,32,1024]{3,2,0,1:T(8,128)(2,1)} %get-tuple-element.3, bf16[4,4,32,1024]{3,2,0,1:T(8,128)(2,1)} %get-tuple-element.4), kind=kOutput, calls=%fused_computation.22 | convolution fusion | flops 541327360 | bytes 6815744 | tf_op jit(solution)/shard_map/secf,efd->secd/dot_general | solution.py:155
  158.9 0.9 copy.91
  159.7 4.1 %all-to-all-start.1 = ((bf16[4,128,512]{2,1,0:T(8,128)(2,1)}), bf16[4,128,512]{2,1,0:T(8,128)(2,1)}, u32[]{:S(2)}, u32[]{:S(2)}) async-start(bf16[4,128,512]{2,1,0:T(8,128)(2,1)} %bitcast.100), calls=%async_computation.3 | async-start | bytes 1048576 | tf_op jit(solution)/shard_map/all_to_all | solution.py:158
  163.9 1.1 copy.93
  165.0 0.3 copy.92
  165.3 1.9 reshape.259
  167.2 0.9 reshape.258
  168.1 0.1 select_reduce_fusion
  168.3 20.2 %reduce-scatter.5.cloned.1.call-done = bf16[64,512]{1,0:T(8,128)(2,1)} async-done(((bf16[64,4096]{1,0:T(8,128)(2,1)}), bf16[64,512]{1,0:T(8,128)(2,1)}) %reduce-scatter.5.cloned.1.call-update) | async-done | bytes 65552 | tf_op jit(solution)/shard_map/reduce_scatter | solution.py:173
  188.4 2.1 %fusion.31 = bf16[64,512]{1,0:T(8,128)(2,1)} fusion(f32[64,512]{1,0:T(8,128)S(1)} %select_reduce_fusion, bf16[512,512]{1,0:T(8,128)(2,1)} %bitcast.22, bf16[64,512]{1,0:T(8,128)(2,1)S(1)} %get-tuple-element.6, bf16[64,512]{1,0:T(8,128)(2,1)} %reduce-scatter.5.cloned.1.call-done), kind=kOutput, calls=%fused_computation.27 | convolution fusion | flops 201490432 | bytes 851968 | tf_op jit(solution)/shard_map/dot_general | solution.py:168
  (46 shorter events, 0.7 us)
Async XLA Ops:
  7.2 14.4 %copy-start = (bf16[256,4096]{1,0:T(8,128)(2,1)S(1)}, bf16[256,4096]{1,0:T(8,128)(2,1)}, u32[]{:S(2)}) copy-start(bf16[256,4096]{1,0:T(8,128)(2,1)} %param.37) | copy-start | bytes 6291460
  7.2 7.0 %copy-start.7 = (f32[16,1024]{1,0:T(8,128)S(1)}, f32[16,1024]{1,0:T(8,128)}, u32[]{:S(2)}) copy-start(f32[16,1024]{1,0:T(8,128)} %param.30) | copy-start | bytes 196612
  7.2 7.1 %copy-start.8 = (f32[16,1024]{1,0:T(8,128)S(1)}, f32[16,1024]{1,0:T(8,128)}, u32[]{:S(2)}) copy-start(f32[16,1024]{1,0:T(8,128)} %param.31) | copy-start | bytes 196612
  7.2 7.2 %copy-start.9 = (f32[16,1024]{1,0:T(8,128)S(1)}, f32[16,1024]{1,0:T(8,128)}, u32[]{:S(2)}) copy-start(f32[16,1024]{1,0:T(8,128)} %param.32) | copy-start | bytes 196612
  7.2 7.9 %copy-start.10 = (f32[16,1024]{1,0:T(8,128)S(1)}, f32[16,1024]{1,0:T(8,128)}, u32[]{:S(2)}) copy-start(f32[16,1024]{1,0:T(8,128)} %param.33) | copy-start | bytes 196612
  7.2 8.0 %copy-start.5 = (f32[64,1024]{1,0:T(8,128)S(1)}, f32[64,1024]{1,0:T(8,128)}, u32[]{:S(2)}) copy-start(f32[64,1024]{1,0:T(8,128)} %param.35) | copy-start | bytes 786436
  7.2 51.3 %reduce-scatter.3.cloned.1.call-start = ((), (), s32[]{:S(2)}) async-start(), calls=%async_computation.4 | async-start | bytes 1179648 | tf_op jit(solution)/shard_map/reduce_scatter | solution.py:116
  11.7 4.4 %copy-start.6 = (f32[64,1024]{1,0:T(8,128)S(1)}, f32[64,1024]{1,0:T(8,128)}, u32[]{:S(2)}) copy-start(f32[64,1024]{1,0:T(8,128)} %param.36) | copy-start | bytes 786436
  17.1 2.5 %copy-start.4 = (f32[16,16,64]{2,1,0:T(8,128)S(1)}, f32[16,16,64]{2,1,0:T(8,128)}, u32[]{:S(2)}) copy-start(f32[16,16,64]{2,1,0:T(8,128)} %reshape.251) | copy-start | bytes 196612
  19.6 3.5 %copy-start.1 = (f32[64,16,64]{2,0,1:T(8,128)}, f32[64,16,64]{2,0,1:T(8,128)S(1)}, u32[]{:S(2)}) copy-start(f32[64,16,64]{2,0,1:T(8,128)S(1)} %get-tuple-element.7) | copy-start | bytes 786436
  21.5 1.6 copy-start.11
  23.1 132.1 %all-reduce.3.cloned.1.call-start = ((), (), s32[]{:S(2)}) async-start(), calls=%async_computation.6 | async-start | bytes 4194304 | tf_op jit(solution)/shard_map/psum | solution.py:152
  85.6 4.0 %copy-start.3 = (bf16[4,512,1024]{2,1,0:T(8,128)(2,1)S(1)}, bf16[4,512,1024]{2,1,0:T(8,128)(2,1)}, u32[]{:S(2)}) copy-start(bf16[4,512,1024]{2,1,0:T(8,128)(2,1)} %param.41) | copy-start | bytes 12582916
  91.4 97.0 %reduce-scatter.5.cloned.1.call-start = ((), (), s32[]{:S(2)}) async-start(), calls=%async_computation.5 | async-start | bytes 589824 | tf_op jit(solution)/shard_map/reduce_scatter | solution.py:173
  158.8 5.0 %copy-start.2 = (f32[64,16,64]{2,0,1:T(8,128)S(1)}, f32[64,16,64]{2,0,1:T(8,128)}, u32[]{:S(2)}) copy-start(f32[64,16,64]{2,0,1:T(8,128)} %copy-done.1) | copy-start | bytes 786436
  159.7 28.7 %all-to-all-start.1 = ((bf16[4,128,512]{2,1,0:T(8,128)(2,1)}), bf16[4,128,512]{2,1,0:T(8,128)(2,1)}, u32[]{:S(2)}, u32[]{:S(2)}) async-start(bf16[4,128,512]{2,1,0:T(8,128)(2,1)} %bitcast.100), calls=%async_computation.3 | async-start | bytes 1048576 | tf_op jit(solution)/shard_map/all_to_all | solution.py:158
  163.9 4.2 %copy-start.12 = (f32[64,4]{0,1:T(4,128)S(1)}, f32[64,4]{0,1:T(4,128)}, u32[]{:S(2)}) copy-start(f32[64,4]{0,1:T(4,128)} %param.45) | copy-start | bytes 3076
Sparse Core Ops, SparseCore 0:
  23.2 35.2 reduce-scatter.2
  91.5 63.6 all-reduce.2
  157.4 30.9 reduce-scatter.4
where the time goes:
time: 198 us; the launch traced here: 197 us
  waiting for transfers between devices  96 us (48%)
  blocking collectives  42.1 us (21%)
  matrix products  24.4 us (12%)
  between operations  14 us (7%)
  local copies, waits for them, and re-layouts  12 us (6%)
  starting transfers between devices  4.25 us (2%)
  other arithmetic  4.21 us (2%)
    psum x1, waiting for transfers between devices, local(): lax.psum(up_part.astype(jnp.bfloat16), 'tp').astype(jnp.float32)  42.7 us
    reduce_scatter x1, waiting for transfers between devices, local(): lax.psum_scatter(mixer_terms, 'tp', scatter_dimension=1, tiled=True)  33.1 us
    reduce_scatter x1, waiting for transfers between devices, local(): lax.psum_scatter(shared_terms.astype(jnp.bfloat16), 'tp', scatter_dimensi...  20.2 us
    all_gather x1, blocking collectives, local(): ffn_rows = lax.all_gather(rows_own, 'tp', axis=1, tiled=True)  16.5 us
    psum x1, blocking collectives, local(): lax.psum(jnp.sum(resid_f * resid_f, axis=1, keepdims=True), 'tp')  13.9 us
    all_to_all x1, blocking collectives, local(): lax.all_to_all(outgoing, 'ep', split_axis=0, concat_axis=0, tiled=True)  11.7 us
    all_to_all x1, starting transfers between devices, local(): lax.all_to_all(expert_terms.reshape(ep_count, expert_dev * capacity, slic...  4.13 us
    dot_general x1, matrix products, local(): jnp.einsum('secd,edf->secf', arrived, expert_up, preferred_element_type=j...  4.04 us
  transfers between devices with their start and end apart: 4, of which 3 were waited for; matrix products, arithmetic and copies ran while one was open for 8% of the time, Pallas kernels for 0%

commit v1 on v0

v1 whole, which is shorter than its diff:
```python
import functools

import jax
import jax.numpy as jnp
from jax import lax
from jax.experimental import pallas as pl
from jax.experimental.pallas import tpu as pltpu
from jax.sharding import PartitionSpec as P

EPS = 1e-06
ROUTED_SCALE = 2.5
F32 = jnp.float32
BF16 = jnp.bfloat16
VMEM_LIMIT = 60 * 1024 * 1024
MESH_ID = pl.DeviceIdType.MESH
IN_VMEM = pl.BlockSpec(memory_space=pltpu.VMEM)


def shift_of(size):
    assert size & (size - 1) == 0
    return size.bit_length() - 1


def split_index(shape, axis, size):
    places = lax.broadcasted_iota(jnp.int32, shape, axis)
    return lax.shift_right_logical(places, shift_of(size))


def mixer_kernel(
    tokens_ref,
    gain_ref,
    w_in_ref,
    decay_ref,
    freq_ref,
    logstep_ref,
    in_re_ref,
    in_im_ref,
    out_re_ref,
    out_im_ref,
    skip_ref,
    old_re_ref,
    old_im_ref,
    w_out_ref,
    terms_ref,
    new_re_ref,
    new_im_ref,
    *,
    groups,
):
    tokens = tokens_ref[...].astype(F32)
    factor = lax.rsqrt(jnp.mean(tokens * tokens, axis=-1, keepdims=True) + EPS)
    normed = (tokens * factor * gain_ref[...]).astype(BF16)
    drive = jnp.dot(normed, w_in_ref[...], preferred_element_type=F32).astype(BF16)
    chan = in_re_ref.shape[0]
    width = decay_ref.shape[1] // groups
    wide = (groups * chan, groups * width)
    own_group = split_index(wide, 0, chan) == split_index(wide, 1, width)

    def spread(ref):
        tiled = jnp.concatenate([ref[...]] * groups, axis=0)
        return jnp.where(own_group, tiled, 0.0).astype(BF16)

    decay, freq = decay_ref[...], freq_ref[...]
    step = jnp.exp(logstep_ref[...])
    mag = jnp.exp(-decay * step)
    pole_re = mag * jnp.cos(freq * step)
    pole_im = mag * jnp.sin(freq * step)
    norm = decay * decay + freq * freq
    diff = pole_re - 1.0
    lift_re = (-decay * diff + freq * pole_im) / norm
    lift_im = (-decay * pole_im - freq * diff) / norm
    push_re = jnp.dot(drive, spread(in_re_ref), preferred_element_type=F32)
    push_im = jnp.dot(drive, spread(in_im_ref), preferred_element_type=F32)
    old_re, old_im = old_re_ref[...], old_im_ref[...]
    new_re = pole_re * old_re - pole_im * old_im + lift_re * push_re - lift_im * push_im
    new_im = pole_re * old_im + pole_im * old_re + lift_re * push_im + lift_im * push_re
    new_re_ref[...] = new_re
    new_im_ref[...] = new_im
    nt = (((1,), (1,)), ((), ()))
    read = lax.dot_general(
        new_re.astype(BF16), spread(out_re_ref), nt, preferred_element_type=F32
    ) - lax.dot_general(new_im.astype(BF16), spread(out_im_ref), nt, preferred_element_type=F32)
    read = read + skip_ref[...] * drive.astype(F32)
    activated = jax.nn.gelu(read).astype(BF16)
    terms_ref[...] = jnp.dot(activated, w_out_ref[...], preferred_element_type=F32).astype(BF16)


def enter(tp, ep, partner, same_core, ep_peers):
    barrier = pltpu.get_barrier_semaphore()
    peers = [{"tp": d} for d in [partner] + same_core] + [{"ep": d} for d in ep_peers]
    for peer in peers:
        pl.semaphore_signal(barrier, inc=1, device_id=peer, device_id_type=MESH_ID)
    pl.semaphore_wait(barrier, len(peers))


def remote(src, dst, send_sem, recv_sem, peer):
    return pltpu.make_async_remote_copy(
        src_ref=src,
        dst_ref=dst,
        send_sem=send_sem,
        recv_sem=recv_sem,
        device_id=peer,
        device_id_type=MESH_ID,
    )


def places(tp_count, ep_count):
    tp, ep = lax.axis_index("tp"), lax.axis_index("ep")
    chips = tp_count // 2
    chip, core = tp // 2, tp % 2
    partner = chip * 2 + (1 - core)
    chip_at = [(chip + d) % chips for d in range(chips)]
    ep_at = [(ep + d) % ep_count for d in range(ep_count)]
    return tp, ep, chip, core, partner, chip_at, ep_at


def scatter_sum(block_of, mate, half, far, sems, where):
    tp, core, partner, chip_at = where
    s1, r1, s2, r2 = sems
    chips = len(chip_at)
    order = list(range(1, chips)) + [0]
    first = {}
    for d in order:
        first[d] = remote(
            block_of(chip_at[d] * 2 + (1 - core)),
            mate.at[d],
            s1.at[d],
            r1.at[d],
            {"tp": partner},
        )
        first[d].start()
    second = {}
    for d in order:
        first[d].wait_recv()
        own = block_of(chip_at[d] * 2 + core)[...].astype(F32) + mate[d].astype(F32)
        half[d] = own.astype(BF16)
        if d:
            second[d] = remote(
                half.at[d], far.at[d], s2.at[d], r2.at[d], {"tp": chip_at[d] * 2 + core}
            )
            second[d].start()

    def finish():
        for d in order:
            first[d].wait_send()
        for d in range(1, chips):
            second[d].wait()

    return finish


def gather_start(own, store, sems, where):
    tp, core, partner, chip_at = where
    s1, r1, s2, r2 = sems
    chips = len(chip_at)
    sends = []
    for d in range(1, chips):
        copy = remote(own, store(tp), s1.at[d], r1.at[d], {"tp": chip_at[d] * 2 + core})
        copy.start()
        sends.append(copy)
    mine = remote(own, store(tp), s2.at[0], r2.at[0], {"tp": partner})
    mine.start()

    def finish():
        passed = [mine]
        for d in range(1, chips):
            sends[d - 1].wait_recv()
            source = chip_at[chips - d] * 2 + core
            onward = remote(store(source), store(source), s2.at[d], r2.at[d], {"tp": partner})
            onward.start()
            passed.append(onward)
        for copy in sends:
            copy.wait_send()
        for copy in passed:
            copy.wait()

    return finish


def resid_kernel(
    terms_ref,
    tokens_ref,
    gain_ref,
    meta_ref,
    ffn_ref,
    resid_ref,
    rows_ref,
    metas_ref,
    mate,
    half,
    far,
    full,
    rows,
    metas,
    rs_s1,
    rs_r1,
    rs_s2,
    rs_r2,
    ag_s1,
    ag_r1,
    ag_s2,
    ag_r2,
    ep_s,
    ep_r,
    meta_s,
    meta_r,
    *,
    tp_count,
    ep_count,
):
    tp, ep, chip, core, partner, chip_at, ep_at = places(tp_count, ep_count)
    enter(tp, ep, partner, [c * 2 + core for c in chip_at[1:]], ep_at[1:])
    where = (tp, core, partner, chip_at)
    slice_width = rows.shape[2]

    def columns(ref):
        return lambda j: ref.at[:, pl.ds(pl.multiple_of(j * slice_width, 128), slice_width)]

    meta_copies = []
    for d in range(1, ep_count):
        copy = remote(meta_ref, metas.at[ep], meta_s.at[d], meta_r.at[d], {"ep": ep_at[d]})
        copy.start()
        meta_copies.append(copy)
    finish = scatter_sum(columns(terms_ref), mate, half, far, (rs_s1, rs_r1, rs_s2, rs_r2), where)
    finish()
    total = half[0].astype(F32)
    for d in range(1, len(chip_at)):
        total = total + far[d].astype(F32)
    resid = (columns(tokens_ref)(tp)[...].astype(F32) + total).astype(BF16)
    resid_ref[...] = resid
    columns(full)(tp)[...] = resid
    gather_start(columns(full)(tp), columns(full), (ag_s1, ag_r1, ag_s2, ag_r2), where)()
    whole = full[...].astype(F32)
    factor = lax.rsqrt(jnp.mean(whole * whole, axis=-1, keepdims=True) + EPS)
    gain_own = columns(gain_ref)(tp)[...]
    rows[ep] = (resid.astype(F32) * factor * gain_own).astype(BF16)
    row_copies = []
    for d in range(1, ep_count):
        copy = remote(rows.at[ep], rows.at[ep], ep_s.at[d], ep_r.at[d], {"ep": ep_at[d]})
        copy.start()
        row_copies.append(copy)
    ffn_ref[...] = (whole * factor * gain_ref[...]).astype(BF16)
    metas[ep] = meta_ref[...]
    for copy in meta_copies + row_copies:
        copy.wait()
    rows_ref[...] = rows[...]
    metas_ref[...] = metas[...]


def slot_map(meta_ref, row, block, base, slots, cap, seqs, values):
    shape = (slots, meta_ref.shape[1])
    slot = lax.broadcasted_iota(jnp.int32, shape, 0)
    same = lax.shift_right_logical(slot, shift_of(cap)) == split_index(shape, 1, seqs)
    wanted = ((slot & (cap - 1)) + base).astype(F32)
    total = jnp.zeros(shape, F32)
    for k in range(row):
        total = total + jnp.where(meta_ref[k : k + 1, :] == wanted, values(k), 0.0)
    return jnp.where(same, total, 0.0)


def up_kernel(meta_ref, rows_ref, gate_ref, up_ref, out_ref, *, top, cap, seqs, width):
    base = pl.program_id(0) * cap
    slots = out_ref.shape[0]
    chosen = slot_map(meta_ref, top, 0, base, slots, cap, seqs, lambda k: 1.0).astype(BF16)
    picked = jnp.dot(chosen, rows_ref[...], preferred_element_type=F32).astype(BF16)
    out_ref[:, :width] = jnp.dot(picked, gate_ref[0], preferred_element_type=F32).astype(BF16)
    out_ref[:, width:] = jnp.dot(picked, up_ref[0], preferred_element_type=F32).astype(BF16)


def down_kernel(meta_ref, inner_ref, down_ref, out_ref, total, *, top, cap, seqs):
    expert = pl.program_id(0)
    slots = inner_ref.shape[0]
    mix = slot_map(
        meta_ref, top, 0, expert * cap, slots, cap, seqs, lambda k: meta_ref[top + k : top + k + 1, :]
    ).astype(BF16)
    terms = jnp.dot(inner_ref[...], down_ref[0], preferred_element_type=F32).astype(BF16)
    part = lax.dot_general(mix, terms, (((0,), (0,)), ((), ())), preferred_element_type=F32)

    @pl.when(expert == 0)
    def _():
        total[...] = part

    @pl.when(expert > 0)
    def _():
        total[...] += part

    out_ref[...] = total[...].astype(BF16)


def inner_kernel(
    parts_ref,
    inner_ref,
    mate,
    half,
    far,
    full,
    rs_s1,
    rs_r1,
    rs_s2,
    rs_r2,
    ag_s1,
    ag_r1,
    ag_s2,
    ag_r2,
    *,
    tp_count,
    ep_count,
):
    tp, ep, chip, core, partner, chip_at, ep_at = places(tp_count, ep_count)
    enter(tp, ep, partner, [c * 2 + core for c in chip_at[1:]], [])
    where = (tp, core, partner, chip_at)
    finish = scatter_sum(
        lambda j: parts_ref.at[j], mate, half, far, (rs_s1, rs_r1, rs_s2, rs_r2), where
    )
    finish()
    total = half[0].astype(F32)
    for d in range(1, len(chip_at)):
        total = total + far[d].astype(F32)
    width = full.shape[2]
    gate, up = total[:, :width], total[:, width:]
    full[tp] = (gate / (1.0 + jnp.exp(-gate)) * up).astype(BF16)
    gather_start(full.at[tp], lambda j: full.at[j], (ag_s1, ag_r1, ag_s2, ag_r2), where)()
    inner_ref[...] = full[...]


def mixed_kernel(
    routed_ref,
    shared_ref,
    resid_ref,
    mixed_ref,
    back,
    mate,
    half,
    far,
    rs_s1,
    rs_r1,
    rs_s2,
    rs_r2,
    ep_s,
    ep_r,
    *,
    tp_count,
    ep_count,
):
    tp, ep, chip, core, partner, chip_at, ep_at = places(tp_count, ep_count)
    enter(tp, ep, partner, [c * 2 + core for c in chip_at[1:]], ep_at[1:])
    where = (tp, core, partner, chip_at)
    slice_width = back.shape[2]
    copies = []
    for d in range(1, ep_count):
        copy = remote(routed_ref.at[ep_at[d]], back.at[d], ep_s.at[d], ep_r.at[d], {"ep": ep_at[d]})
        copy.start()
        copies.append(copy)

    def columns(j):
        return shared_ref.at[:, pl.ds(pl.multiple_of(j * slice_width, 128), slice_width)]

    finish = scatter_sum(columns, mate, half, far, (rs_s1, rs_r1, rs_s2, rs_r2), where)
    finish()
    total = resid_ref[...].astype(F32) + half[0].astype(F32)
    for d in range(1, len(chip_at)):
        total = total + far[d].astype(F32)
    total = total + routed_ref[ep].astype(F32)
    for copy in copies:
        copy.wait()
    for d in range(1, ep_count):
        total = total + back[d].astype(F32)
    mixed_ref[...] = total.astype(BF16)


def local(
    tokens,
    norm_gain,
    ffn_gain,
    w_in,
    decay_rate,
    frequency,
    log_step,
    input_real,
    input_imag,
    readout_real,
    readout_imag,
    skip_gain,
    state_real,
    state_imag,
    w_out,
    shared_gate,
    shared_up,
    shared_down,
    expert_gate,
    expert_up,
    expert_down,
    routing,
    route_weight,
):
    seq_count, model_width = tokens.shape
    tp_count = lax.axis_size("tp")
    ep_count = lax.axis_size("ep")
    chips = tp_count // 2
    slice_width = model_width // tp_count
    groups = log_step.shape[0]
    modes = decay_rate.shape[0]
    expert_dev, _, hidden = expert_gate.shape
    expert_count = expert_dev * ep_count
    top_count = routing.shape[1]
    capacity = 2 * seq_count * top_count // expert_count
    slots = ep_count * capacity
    slot_count = expert_dev * slots
    own_slots = slot_count // tp_count
    dma = pltpu.SemaphoreType.DMA
    tp_sems = [dma((chips,))] * 4
    local_params = pltpu.CompilerParams(vmem_limit_bytes=VMEM_LIMIT)

    def talk(number):
        return pltpu.CompilerParams(
            collective_id=number, has_side_effects=True, vmem_limit_bytes=VMEM_LIMIT
        )

    flat_ids = routing.T.reshape(-1)
    one_hot = (flat_ids[:, None] == jnp.arange(expert_count, dtype=jnp.int32)[None, :]).astype(BF16)
    count = flat_ids.shape[0]
    before = jnp.arange(count)[:, None] > jnp.arange(count)[None, :]
    earlier = jnp.dot(before.astype(BF16), one_hot, preferred_element_type=F32)
    rank = jnp.sum(earlier * one_hot.astype(F32), axis=1)
    target = (flat_ids * capacity).astype(F32) + rank
    weights = route_weight / jnp.sum(route_weight, axis=1, keepdims=True) * ROUTED_SCALE
    meta = jnp.concatenate([target.reshape(top_count, seq_count), weights.T], axis=0)

    terms, new_real, new_imag = pl.pallas_call(
        functools.partial(mixer_kernel, groups=groups),
        out_shape=(
            jax.ShapeDtypeStruct((seq_count, model_width), BF16),
            jax.ShapeDtypeStruct((seq_count, modes), F32),
            jax.ShapeDtypeStruct((seq_count, modes), F32),
        ),
        in_specs=[IN_VMEM] * 14,
        out_specs=(IN_VMEM,) * 3,
        compiler_params=local_params,
        name="mixer",
    )(
        tokens,
        norm_gain[None, :],
        w_in,
        decay_rate[None, :],
        frequency[None, :],
        jnp.repeat(log_step, modes // groups)[None, :],
        input_real,
        input_imag,
        readout_real,
        readout_imag,
        skip_gain[None, :],
        state_real,
        state_imag,
        w_out,
    )
    block = (seq_count, slice_width)
    ffn_rows, resid_own, rows_all, metas = pl.pallas_call(
        functools.partial(resid_kernel, tp_count=tp_count, ep_count=ep_count),
        out_shape=(
            jax.ShapeDtypeStruct((seq_count, model_width), BF16),
            jax.ShapeDtypeStruct(block, BF16),
            jax.ShapeDtypeStruct((ep_count,) + block, BF16),
            jax.ShapeDtypeStruct((ep_count,) + meta.shape, F32),
        ),
        in_specs=[IN_VMEM] * 4,
        out_specs=(IN_VMEM,) * 4,
        scratch_shapes=[
            pltpu.VMEM((chips,) + block, BF16),
            pltpu.VMEM((chips,) + block, BF16),
            pltpu.VMEM((chips,) + block, BF16),
            pltpu.VMEM((seq_count, model_width), BF16),
            pltpu.VMEM((ep_count,) + block, BF16),
            pltpu.VMEM((ep_count,) + meta.shape, F32),
        ]
        + tp_sems
        + tp_sems
        + [dma((ep_count,))] * 4,
        compiler_params=talk(1),
        name="resid",
    )(terms, tokens, ffn_gain[None, :], meta)

    first_slot = (lax.axis_index("ep") * (expert_dev * capacity)).astype(F32)
    flat_meta = jnp.swapaxes(metas, 0, 1).reshape(meta.shape[0], ep_count * seq_count)
    flat_meta = flat_meta - jnp.where(jnp.arange(meta.shape[0])[:, None] < top_count, first_slot, 0.0)
    whole = lambda shape: pl.BlockSpec(shape, lambda e: (0,) * len(shape))
    parts = pl.pallas_call(
        functools.partial(up_kernel, top=top_count, cap=capacity, seqs=seq_count, width=hidden),
        out_shape=jax.ShapeDtypeStruct((slot_count, 2 * hidden), BF16),
        grid=(expert_dev,),
        in_specs=[
            whole(flat_meta.shape),
            whole((ep_count * seq_count, slice_width)),
            pl.BlockSpec((1, slice_width, hidden), lambda e: (e, 0, 0)),
            pl.BlockSpec((1, slice_width, hidden), lambda e: (e, 0, 0)),
        ],
        out_specs=pl.BlockSpec((slots, 2 * hidden), lambda e: (e, 0)),
        compiler_params=local_params,
        name="gate_up",
    )(flat_meta, rows_all.reshape(ep_count * seq_count, slice_width), expert_gate, expert_up)

    inner = pl.pallas_call(
        functools.partial(inner_kernel, tp_count=tp_count, ep_count=ep_count),
        out_shape=jax.ShapeDtypeStruct((tp_count, own_slots, hidden), BF16),
        in_specs=[IN_VMEM],
        out_specs=IN_VMEM,
        scratch_shapes=[pltpu.VMEM((chips, own_slots, 2 * hidden), BF16)] * 3
        + [pltpu.VMEM((tp_count, own_slots, hidden), BF16)]
        + tp_sems
        + tp_sems,
        compiler_params=talk(2),
        name="inner",
    )(parts.reshape(tp_count, own_slots, 2 * hidden))

    shared_gate_rows = jnp.dot(ffn_rows, shared_gate, preferred_element_type=F32)
    shared_up_rows = jnp.dot(ffn_rows, shared_up, preferred_element_type=F32)
    shared_inner = (jax.nn.silu(shared_gate_rows) * shared_up_rows).astype(BF16)
    shared_terms = jnp.dot(shared_inner, shared_down, preferred_element_type=F32).astype(BF16)

    routed = pl.pallas_call(
        functools.partial(down_kernel, top=top_count, cap=capacity, seqs=seq_count),
        out_shape=jax.ShapeDtypeStruct((ep_count * seq_count, slice_width), BF16),
        grid=(expert_dev,),
        in_specs=[
            whole(flat_meta.shape),
            pl.BlockSpec((slots, hidden), lambda e: (e, 0)),
            pl.BlockSpec((1, hidden, slice_width), lambda e: (e, 0, 0)),
        ],
        out_specs=whole((ep_count * seq_count, slice_width)),
        scratch_shapes=[pltpu.VMEM((ep_count * seq_count, slice_width), F32)],
        compiler_params=local_params,
        name="down",
    )(flat_meta, inner.reshape(slot_count, hidden), expert_down)

    mixed = pl.pallas_call(
        functools.partial(mixed_kernel, tp_count=tp_count, ep_count=ep_count),
        out_shape=jax.ShapeDtypeStruct(block, BF16),
        in_specs=[IN_VMEM] * 3,
        out_specs=IN_VMEM,
        scratch_shapes=[pltpu.VMEM((ep_count,) + block, BF16)]
        + [pltpu.VMEM((chips,) + block, BF16)] * 3
        + tp_sems
        + [dma((ep_count,))] * 2,
        compiler_params=talk(3),
        name="mixed",
    )(routed.reshape((ep_count,) + block), shared_terms, resid_own)
    return (mixed, new_real, new_imag)


def solution(mesh):
    placed = (
        P("ep", None),
        P(),
        P(),
        P(None, "tp"),
        P("tp"),
        P("tp"),
        P("tp"),
        P(None, "tp"),
        P(None, "tp"),
        P(None, "tp"),
        P(None, "tp"),
        P("tp"),
        P("ep", "tp"),
        P("ep", "tp"),
        P("tp", None),
        P(None, "tp"),
        P(None, "tp"),
        P("tp", None),
        P("ep", "tp", None),
        P("ep", "tp", None),
        P("ep", None, "tp"),
        P("ep", None),
        P("ep", None),
    )
    return jax.shard_map(
        local,
        mesh=mesh,
        in_specs=placed,
        out_specs=(P("ep", "tp"), P("ep", "tp"), P("ep", "tp")),
        check_vma=False,
    )
```

time: 198 us -> 117 us (0.59)
  Pallas kernels: 0 us -> 104 us
  waiting for transfers between devices: 96 us -> 0 us
  blocking collectives: 42.1 us -> 0 us
  matrix products: 24.4 us -> 3.97 us
  between operations: 14 us -> 0.72 us
  local copies, waits for them, and re-layouts: 12 us -> 4.54 us
  starting transfers between devices: 4.25 us -> 0 us
    pallas_call x0 -> x6, Pallas kernels: none -> 104 us  [the longest x1 43.8 us: local(): pl.pallas_call(functools.partial(inner_kernel, tp_count=tp_count, ep_coun...]
    reduce_scatter x2 -> x0, waiting for transfers between devices: 53.2 us -> none  [the longest x1 33.1 us: local(): lax.psum_scatter(mixer_terms, 'tp', scatter_dimension=1, tiled=True)]
    psum x1 -> x0, waiting for transfers between devices: 42.7 us -> none  [local(): lax.psum(up_part.astype(jnp.bfloat16), 'tp').astype(jnp.float32)]
    dot_general x13 -> x3, matrix products: 24.4 us -> 3.97 us  [the longest x1 2.42 us: local(): jnp.dot(shared_inner, shared_down, preferred_element_type=F32).astype(BF16)]
    all_gather x1 -> x0, blocking collectives: 16.5 us -> none  [local(): ffn_rows = lax.all_gather(rows_own, 'tp', axis=1, tiled=True)]
    psum x1 -> x0, blocking collectives: 13.9 us -> none  [local(): lax.psum(jnp.sum(resid_f * resid_f, axis=1, keepdims=True), 'tp')]
    all_to_all x1 -> x0, blocking collectives: 11.7 us -> none  [local(): lax.all_to_all(outgoing, 'ep', split_axis=0, concat_axis=0, tiled=True)]
    reshape x9 -> x1, local copies, waits for them, and re-layouts: 6.42 us -> 0.08 us  [local(): jnp.swapaxes(metas, 0, 1).reshape(meta.shape[0], ep_count * seq_count)]
  transfers between devices with their start and end apart: 4 -> 0, of which waited for: 3 -> 0; matrix products, arithmetic and copies ran while one was open for 8% -> 0% of each run, Pallas kernels for 0% -> 0%
where the time goes in v1:
time: 117 us; the launch traced here: 116 us
  Pallas kernels  104 us (89%)
  local copies, waits for them, and re-layouts  4.54 us (4%)
  matrix products  3.97 us (3%)
  other arithmetic  3.53 us (3%)
    pallas_call x1, Pallas kernels, local(): pl.pallas_call(functools.partial(inner_kernel, tp_count=tp_count, ep_coun...  43.8 us
    pallas_call x1, Pallas kernels, local(): pl.pallas_call(functools.partial(resid_kernel, tp_count=tp_count, ep_coun...  27.7 us
    pallas_call x1, Pallas kernels, local(): pl.pallas_call(functools.partial(mixed_kernel, tp_count=tp_count, ep_coun...  15.2 us
    pallas_call x1, Pallas kernels, local(): pl.pallas_call(functools.partial(up_kernel, top=top_count, cap=capacity,...  6.18 us
    pallas_call x1, Pallas kernels, local(): pl.pallas_call(functools.partial(mixer_kernel, groups=groups), out_shape=...  5.58 us
    pallas_call x1, Pallas kernels, local(): pl.pallas_call(functools.partial(down_kernel, top=top_count, cap=capacity...  5.16 us
    dot_general x1, matrix products, local(): jnp.dot(shared_inner, shared_down, preferred_element_type=F32).astype(BF16)  2.42 us

profile of v1, /device:TPU:0, one launch (start us, length us, event | category | flops | bytes accessed | tf_op | source)
XLA Modules:
  0.0 116.4 jit_solution(11155943125228790062)
XLA Ops:
  0.6 0.0 copy-start
  0.6 0.0 copy-start.2
  0.7 0.8 reduce_sum.22
  1.5 0.8 eq.15
  2.3 0.0 copy-start.1
  2.3 0.2 fusion.1
  2.5 0.1 reduce_sum.21
  2.6 0.7 convert_add_fusion
  3.3 0.7 multiply_bitcast_fusion
  4.0 0.6 pad_maximum_fusion.meta_ref
  4.6 0.7 broadcast_in_dim.34
  5.3 0.7 broadcast_in_dim_reshape.4.logstep_ref
  6.0 5.6 %mixer.1 = (bf16[64,4096]{1,0:T(8,128)(2,1)}, f32[64,1024]{1,0:T(8,128)}, f32[64,1024]{1,0:T(8,128)}) custom-call(bf16[64,4096]{1,0:T(8,128)(2,1)} %tokens_ref.3, f32[1,4096]{1,0:T(1,128)} %bitcast.23, bf16[4096,256]{1,0:T(8,128)(2,1)} %w_in_ref.1, f32[1,1024]{1,0:T(1,128)} %bitcast.27, f32[1,1024]{1,0:T(1,128)} %bitcast.28, ...), custom_call_target="tpu_custom_call" | custom-call | tf_op jit(solution)/shard_map/mixer/pallas_call | solution.py:429
  11.6 27.7 %resid.1 = (bf16[64,4096]{1,0:T(8,128)(2,1)}, bf16[64,512]{1,0:T(8,128)(2,1)}, bf16[4,64,512]{2,1,0:T(8,128)(2,1)}, f32[4,8,64]{2,1,0:T(8,128)}) custom-call(bf16[64,4096]{1,0:T(8,128)(2,1)} %get-tuple-element.10.terms_ref, bf16[64,4096]{1,0:T(8,128)(2,1)} %tokens_ref.3, f32[1,4096]{1,0:T(1,128)} %bitcast.24, f32[8,64]{1,0:T(8,128)} %pad_maximum_fusion.meta_ref), custom_call_target="tpu_custom_call" | custom-call | tf_op jit(solution)/shard_map/resid/pallas_call | solution.py:457
  39.3 0.7 copy.26
  40.0 0.1 reshape.33
  40.1 0.7 broadcast_subtract_fusion.meta_ref
  40.7 0.0 copy-done.2
  40.7 1.4 %fusion.11 = f32[64,128]{1,0:T(8,128)S(1)} fusion(bf16[64,4096]{1,0:T(8,128)(2,1)} %get-tuple-element.13, bf16[4096,128]{1,0:T(8,128)(2,1)S(1)} %copy-done.2), kind=kOutput, calls=%fused_computation.21 | convolution fusion | flops 67108864 | bytes 1605632 | tf_op jit(solution)/shard_map/dot_general | solution.py:514
  42.1 0.0 copy-done
  42.1 0.0 copy-done.1
  42.1 2.4 %convolution_convert_fusion.shared_ref = bf16[64,4096]{1,0:T(8,128)(2,1)} fusion(bf16[128,4096]{1,0:T(8,128)(2,1)S(1)} %copy-done, bf16[64,4096]{1,0:T(8,128)(2,1)} %get-tuple-element.13, bf16[4096,128]{1,0:T(8,128)(2,1)S(1)} %copy-done.1, f32[64,128]{1,0:T(8,128)S(1)} %fusion.11), kind=kOutput, calls=%fused_computation | convolution fusion | flops 134529024 | bytes 3178496 | tf_op jit(solution)/shard_map/dot_general | solution.py:517
  44.5 6.2 %gate_up.1 = bf16[512,2048]{1,0:T(8,128)(2,1)} custom-call(f32[8,256]{1,0:T(8,128)} %broadcast_subtract_fusion.meta_ref, bf16[256,512]{1,0:T(8,128)(2,1)} %bitcast.22, bf16[4,512,1024]{2,1,0:T(8,128)(2,1)} %gate_ref.1, bf16[4,512,1024]{2,1,0:T(8,128)(2,1)} %up_ref.1), custom_call_target="tpu_custom_call" | custom-call | tf_op jit(solution)/shard_map/gate_up/pallas_call | solution.py:486
  50.7 43.8 %inner.1 = bf16[8,64,1024]{2,1,0:T(8,128)(2,1)} custom-call(bf16[8,64,2048]{2,1,0:T(8,128)(2,1)} %bitcast.19), custom_call_target="tpu_custom_call" | custom-call | tf_op jit(solution)/shard_map/inner/pallas_call | solution.py:501
  94.6 5.2 %down.1 = bf16[256,512]{1,0:T(8,128)(2,1)} custom-call(f32[8,256]{1,0:T(8,128)} %broadcast_subtract_fusion.meta_ref, bf16[512,1024]{1,0:T(8,128)(2,1)} %bitcast.20, bf16[4,1024,512]{2,1,0:T(8,128)(2,1)} %down_ref.1), custom_call_target="tpu_custom_call" | custom-call | tf_op jit(solution)/shard_map/down/pallas_call | solution.py:519
  99.7 15.2 %mixed.1 = bf16[64,512]{1,0:T(8,128)(2,1)} custom-call(bf16[4,64,512]{2,1,0:T(8,128)(2,1)} %bitcast.21, bf16[64,4096]{1,0:T(8,128)(2,1)} %convolution_convert_fusion.shared_ref, bf16[64,512]{1,0:T(8,128)(2,1)} %get-tuple-element.14.resid_ref), custom_call_target="tpu_custom_call" | custom-call | tf_op jit(solution)/shard_map/mixed/pallas_call | solution.py:534
  114.9 1.5 %copy.28 = bf16[64,512]{1,0:T(8,128)(2,1)} copy(bf16[64,512]{1,0:T(8,128)(2,1)} %mixed.1) | data formatting | bytes 131072
  (1 shorter events, 0.0 us)
Async XLA Ops:
  0.6 41.5 %copy-start = (bf16[128,4096]{1,0:T(8,128)(2,1)S(1)}, bf16[128,4096]{1,0:T(8,128)(2,1)}, u32[]{:S(2)}) copy-start(bf16[128,4096]{1,0:T(8,128)(2,1)} %param.40) | copy-start | bytes 3145732
  0.6 40.1 %copy-start.2 = (bf16[4096,128]{1,0:T(8,128)(2,1)S(1)}, bf16[4096,128]{1,0:T(8,128)(2,1)}, u32[]{:S(2)}) copy-start(bf16[4096,128]{1,0:T(8,128)(2,1)} %param.38) | copy-start | bytes 3145732
  2.3 39.8 %copy-start.1 = (bf16[4096,128]{1,0:T(8,128)(2,1)S(1)}, bf16[4096,128]{1,0:T(8,128)(2,1)}, u32[]{:S(2)}) copy-start(bf16[4096,128]{1,0:T(8,128)(2,1)} %param.39) | copy-start | bytes 3145732

commit v2 on v1

--- a/solution.py
+++ b/solution.py
@@ -11,7 +11,7 @@
 ROUTED_SCALE = 2.5
 F32 = jnp.float32
 BF16 = jnp.bfloat16
-VMEM_LIMIT = 60 * 1024 * 1024
+VMEM_LIMIT = 20 * 1024 * 1024
 MESH_ID = pl.DeviceIdType.MESH
 IN_VMEM = pl.BlockSpec(memory_space=pltpu.VMEM)
 
@@ -41,12 +41,34 @@
     old_re_ref,
     old_im_ref,
     w_out_ref,
+    ids_ref,
+    share_ref,
     terms_ref,
     new_re_ref,
     new_im_ref,
+    meta_ref,
     *,
     groups,
+    experts,
+    cap,
 ):
+    top, seqs = ids_ref.shape
+    square = (seqs, seqs)
+    before = (
+        lax.broadcasted_iota(jnp.int32, square, 0) < lax.broadcasted_iota(jnp.int32, square, 1)
+    ).astype(BF16)
+    named = lax.broadcasted_iota(jnp.int32, (experts, seqs), 0)
+    taken = jnp.zeros((experts, 1), F32)
+    shares = share_ref[...]
+    scale = ROUTED_SCALE / jnp.sum(shares, axis=0, keepdims=True)
+    for k in range(top):
+        ids = ids_ref[k : k + 1, :]
+        hot = (named == ids).astype(F32)
+        earlier = jnp.dot(hot.astype(BF16), before, preferred_element_type=F32) + taken
+        rank = jnp.sum(earlier * hot, axis=0, keepdims=True)
+        taken = taken + jnp.sum(hot, axis=1, keepdims=True)
+        meta_ref[k : k + 1, :] = (ids * cap).astype(F32) + rank
+        meta_ref[top + k : top + k + 1, :] = shares[k : k + 1, :] * scale
     tokens = tokens_ref[...].astype(F32)
     factor = lax.rsqrt(jnp.mean(tokens * tokens, axis=-1, keepdims=True) + EPS)
     normed = (tokens * factor * gain_ref[...]).astype(BF16)
@@ -61,7 +83,13 @@
         return jnp.where(own_group, tiled, 0.0).astype(BF16)
 
     decay, freq = decay_ref[...], freq_ref[...]
-    step = jnp.exp(logstep_ref[...])
+    over = (groups, groups * width)
+    member = lax.broadcasted_iota(jnp.int32, over, 0) == split_index(over, 1, width)
+    column = jnp.sum(jnp.where(
+        lax.broadcasted_iota(jnp.int32, (groups, groups), 0)
+        == lax.broadcasted_iota(jnp.int32, (groups, groups), 1), logstep_ref[...], 0.0,
+    ), axis=1, keepdims=True)
+    step = jnp.exp(jnp.sum(jnp.where(member, column, 0.0), axis=0, keepdims=True))
     mag = jnp.exp(-decay * step)
     pole_re = mag * jnp.cos(freq * step)
     pole_im = mag * jnp.sin(freq * step)
@@ -130,6 +158,14 @@
         )
         first[d].start()
     second = {}
+    return functools.partial(scatter_second, block_of, mate, half, far, sems, where, first, second)
+
+
+def scatter_second(block_of, mate, half, far, sems, where, first, second):
+    tp, core, partner, chip_at = where
+    s1, r1, s2, r2 = sems
+    chips = len(chip_at)
+    order = list(range(1, chips)) + [0]
     for d in order:
         first[d].wait_recv()
         own = block_of(chip_at[d] * 2 + core)[...].astype(F32) + mate[d].astype(F32)
@@ -207,6 +243,7 @@
     *,
     tp_count,
     ep_count,
+    first_step,
 ):
     tp, ep, chip, core, partner, chip_at, ep_at = places(tp_count, ep_count)
     enter(tp, ep, partner, [c * 2 + core for c in chip_at[1:]], ep_at[1:])
@@ -221,8 +258,7 @@
         copy = remote(meta_ref, metas.at[ep], meta_s.at[d], meta_r.at[d], {"ep": ep_at[d]})
         copy.start()
         meta_copies.append(copy)
-    finish = scatter_sum(columns(terms_ref), mate, half, far, (rs_s1, rs_r1, rs_s2, rs_r2), where)
-    finish()
+    scatter_sum(columns(terms_ref), mate, half, far, (rs_s1, rs_r1, rs_s2, rs_r2), where)()()
     total = half[0].astype(F32)
     for d in range(1, len(chip_at)):
         total = total + far[d].astype(F32)
@@ -244,7 +280,10 @@
     for copy in meta_copies + row_copies:
         copy.wait()
     rows_ref[...] = rows[...]
-    metas_ref[...] = metas[...]
+    flat = jnp.concatenate([metas[b] for b in range(ep_count)], axis=1)
+    base = (ep * first_step).astype(F32)
+    row = lax.broadcasted_iota(jnp.int32, flat.shape, 0)
+    metas_ref[...] = flat - jnp.where(row < flat.shape[0] // 2, base, 0.0)
 
 
 def slot_map(meta_ref, row, block, base, slots, cap, seqs, values):
@@ -289,78 +328,185 @@
 
 def inner_kernel(
     parts_ref,
+    ffn_ref,
+    shared_gate_ref,
+    shared_up_ref,
+    shared_down_ref,
     inner_ref,
+    shared_ref,
     mate,
-    half,
-    far,
+    inbox,
+    outbox,
     full,
+    terms,
+    s_mate,
+    s_half,
+    s_far,
+    m_s,
+    m_r,
+    c_s,
+    c_r,
+    g_s,
+    g_r,
+    p_s,
+    p_r,
     rs_s1,
     rs_r1,
     rs_s2,
     rs_r2,
-    ag_s1,
-    ag_r1,
-    ag_s2,
-    ag_r2,
     *,
     tp_count,
     ep_count,
 ):
     tp, ep, chip, core, partner, chip_at, ep_at = places(tp_count, ep_count)
+    chips = tp_count // 2
+    pieces = full.shape[2]
+    width = full.shape[4]
+    other = 1 - core
     enter(tp, ep, partner, [c * 2 + core for c in chip_at[1:]], [])
-    where = (tp, core, partner, chip_at)
-    finish = scatter_sum(
-        lambda j: parts_ref.at[j], mate, half, far, (rs_s1, rs_r1, rs_s2, rs_r2), where
+    stage = [chips - 1 - chip, chip]
+    ahead = [(chip - 1) * 2 + core, (chip + 1) * 2 + core]
+    back = [(chip + 1) * 2 + core, (chip - 1) * 2 + core]
+
+    def to_mate(h, k):
+        return remote(
+            parts_ref.at[h, other, k], mate.at[h, k], m_s.at[h, k], m_r.at[h, k], {"tp": partner}
+        )
+
+    def to_ahead(h, k):
+        return remote(
+            outbox.at[h, k], inbox.at[h, k], c_s.at[h, k], c_r.at[h, k], {"tp": ahead[h]}
+        )
+
+    def to_back(h, k):
+        piece = full.at[h, core, k]
+        return remote(piece, piece, g_s.at[h, k], g_r.at[h, k], {"tp": back[h]})
+
+    def to_partner(h, k):
+        piece = full.at[h, core, k]
+        return remote(piece, piece, p_s.at[h, k], p_r.at[h, k], {"tp": partner})
+
+    def sum_step(h, k):
+        to_mate(h, k).wait_recv()
+        own = parts_ref[h, core, k].astype(F32) + mate[h, k].astype(F32)
+
+        @pl.when(stage[h] == 0)
+        def _():
+            outbox[h, k] = own.astype(BF16)
+
+        @pl.when(stage[h] > 0)
+        def _():
+            to_ahead(h, k).wait_recv()
+            total = own + inbox[h, k].astype(F32)
+
+            @pl.when(stage[h] < chips - 1)
+            def _():
+                outbox[h, k] = total.astype(BF16)
+
+            @pl.when(stage[h] == chips - 1)
+            def _():
+                gate, up = total[:, :width], total[:, width:]
+                full[h, core, k] = (gate / (1.0 + jnp.exp(-gate)) * up).astype(BF16)
+                to_back(h, k).start()
+                to_partner(h, k).start()
+
+        @pl.when(stage[h] < chips - 1)
+        def _():
+            to_ahead(h, k).start()
+
+    def pass_step(h, k):
+        to_back(h, k).wait_recv()
+
+        @pl.when(stage[h] > 0)
+        def _():
+            to_back(h, k).start()
+
+        to_partner(h, k).start()
+
+    gap = 2
+
+    def one_step(i):
+        for h in range(2):
+            k = i - gap * stage[h]
+
+            @pl.when((k >= 0) & (k < pieces))
+            def _():
+                sum_step(h, k)
+
+        for h in range(2):
+            late = i - gap * (chips - 1) - gap * (chips - 1 - stage[h])
+
+            @pl.when((stage[h] < chips - 1) & (late >= 0) & (late < pieces))
+            def _():
+                pass_step(h, late)
+
+    def steps(low, high):
+        @pl.loop(low, high)
+        def _(i):
+            one_step(i)
+
+    @pl.loop(0, pieces)
+    def _(k):
+        for h in range(2):
+            to_mate(h, k).start()
+
+    total_steps = pieces + 2 * gap * (chips - 1)
+    steps(0, 3)
+    rows = ffn_ref[...]
+    gate = jnp.dot(rows, shared_gate_ref[...], preferred_element_type=F32)
+    up = jnp.dot(rows, shared_up_ref[...], preferred_element_type=F32)
+    hidden = (gate / (1.0 + jnp.exp(-gate)) * up).astype(BF16)
+    terms[...] = jnp.dot(hidden, shared_down_ref[...], preferred_element_type=F32).astype(BF16)
+    slice_width = s_half.shape[2]
+
+    def columns(j):
+        return terms.at[:, pl.ds(pl.multiple_of(j * slice_width, 128), slice_width)]
+
+    second = scatter_sum(
+        columns, s_mate, s_half, s_far, (rs_s1, rs_r1, rs_s2, rs_r2),
+        (tp, core, partner, chip_at),
     )
+    middle = gap * (chips - 1) + 2
+    steps(3, middle)
+    finish = second()
+    steps(middle, total_steps)
     finish()
-    total = half[0].astype(F32)
-    for d in range(1, len(chip_at)):
-        total = total + far[d].astype(F32)
-    width = full.shape[2]
-    gate, up = total[:, :width], total[:, width:]
-    full[tp] = (gate / (1.0 + jnp.exp(-gate)) * up).astype(BF16)
-    gather_start(full.at[tp], lambda j: full.at[j], (ag_s1, ag_r1, ag_s2, ag_r2), where)()
+    shared = s_half[0].astype(F32)
+    for d in range(1, chips):
+        shared = shared + s_far[d].astype(F32)
+    shared_ref[...] = shared
+
+    @pl.loop(0, pieces)
+    def _(k):
+        for h in range(2):
+            to_mate(h, k).wait_send()
+            to_partner(h, k).wait()
+
+            @pl.when(stage[h] < chips - 1)
+            def _():
+                to_ahead(h, k).wait_send()
+
+            @pl.when(stage[h] > 0)
+            def _():
+                to_back(h, k).wait_send()
+
     inner_ref[...] = full[...]
 
 
 def mixed_kernel(
-    routed_ref,
-    shared_ref,
-    resid_ref,
-    mixed_ref,
-    back,
-    mate,
-    half,
-    far,
-    rs_s1,
-    rs_r1,
-    rs_s2,
-    rs_r2,
-    ep_s,
-    ep_r,
-    *,
-    tp_count,
-    ep_count,
+    routed_ref, shared_ref, resid_ref, mixed_ref, back, ep_s, ep_r, *, tp_count, ep_count
 ):
     tp, ep, chip, core, partner, chip_at, ep_at = places(tp_count, ep_count)
-    enter(tp, ep, partner, [c * 2 + core for c in chip_at[1:]], ep_at[1:])
-    where = (tp, core, partner, chip_at)
-    slice_width = back.shape[2]
+    barrier = pltpu.get_barrier_semaphore()
+    for peer in ep_at[1:]:
+        pl.semaphore_signal(barrier, inc=1, device_id={"ep": peer}, device_id_type=MESH_ID)
+    pl.semaphore_wait(barrier, ep_count - 1)
     copies = []
     for d in range(1, ep_count):
         copy = remote(routed_ref.at[ep_at[d]], back.at[d], ep_s.at[d], ep_r.at[d], {"ep": ep_at[d]})
         copy.start()
         copies.append(copy)
-
-    def columns(j):
-        return shared_ref.at[:, pl.ds(pl.multiple_of(j * slice_width, 128), slice_width)]
-
-    finish = scatter_sum(columns, mate, half, far, (rs_s1, rs_r1, rs_s2, rs_r2), where)
-    finish()
-    total = resid_ref[...].astype(F32) + half[0].astype(F32)
-    for d in range(1, len(chip_at)):
-        total = total + far[d].astype(F32)
-    total = total + routed_ref[ep].astype(F32)
+    total = resid_ref[...].astype(F32) + shared_ref[...] + routed_ref[ep].astype(F32)
     for copy in copies:
         copy.wait()
     for d in range(1, ep_count):
@@ -406,35 +552,25 @@
     capacity = 2 * seq_count * top_count // expert_count
     slots = ep_count * capacity
     slot_count = expert_dev * slots
-    own_slots = slot_count // tp_count
     dma = pltpu.SemaphoreType.DMA
     tp_sems = [dma((chips,))] * 4
     local_params = pltpu.CompilerParams(vmem_limit_bytes=VMEM_LIMIT)
 
-    def talk(number):
+    def talk(number, mib):
         return pltpu.CompilerParams(
-            collective_id=number, has_side_effects=True, vmem_limit_bytes=VMEM_LIMIT
+            collective_id=number, has_side_effects=True, vmem_limit_bytes=mib * 1024 * 1024
         )
 
-    flat_ids = routing.T.reshape(-1)
-    one_hot = (flat_ids[:, None] == jnp.arange(expert_count, dtype=jnp.int32)[None, :]).astype(BF16)
-    count = flat_ids.shape[0]
-    before = jnp.arange(count)[:, None] > jnp.arange(count)[None, :]
-    earlier = jnp.dot(before.astype(BF16), one_hot, preferred_element_type=F32)
-    rank = jnp.sum(earlier * one_hot.astype(F32), axis=1)
-    target = (flat_ids * capacity).astype(F32) + rank
-    weights = route_weight / jnp.sum(route_weight, axis=1, keepdims=True) * ROUTED_SCALE
-    meta = jnp.concatenate([target.reshape(top_count, seq_count), weights.T], axis=0)
-
-    terms, new_real, new_imag = pl.pallas_call(
-        functools.partial(mixer_kernel, groups=groups),
+    terms, new_real, new_imag, meta = pl.pallas_call(
+        functools.partial(mixer_kernel, groups=groups, experts=expert_count, cap=capacity),
         out_shape=(
             jax.ShapeDtypeStruct((seq_count, model_width), BF16),
             jax.ShapeDtypeStruct((seq_count, modes), F32),
             jax.ShapeDtypeStruct((seq_count, modes), F32),
+            jax.ShapeDtypeStruct((2 * top_count, seq_count), F32),
         ),
-        in_specs=[IN_VMEM] * 14,
-        out_specs=(IN_VMEM,) * 3,
+        in_specs=[IN_VMEM] * 16,
+        out_specs=(IN_VMEM,) * 4,
         compiler_params=local_params,
         name="mixer",
     )(
@@ -443,7 +579,7 @@
         w_in,
         decay_rate[None, :],
         frequency[None, :],
-        jnp.repeat(log_step, modes // groups)[None, :],
+        log_step[None, :],
         input_real,
         input_imag,
         readout_real,
@@ -452,15 +588,19 @@
         state_real,
         state_imag,
         w_out,
+        routing.T,
+        route_weight.T,
     )
     block = (seq_count, slice_width)
-    ffn_rows, resid_own, rows_all, metas = pl.pallas_call(
-        functools.partial(resid_kernel, tp_count=tp_count, ep_count=ep_count),
+    ffn_rows, resid_own, rows_all, flat_meta = pl.pallas_call(
+        functools.partial(
+            resid_kernel, tp_count=tp_count, ep_count=ep_count, first_step=expert_dev * capacity
+        ),
         out_shape=(
             jax.ShapeDtypeStruct((seq_count, model_width), BF16),
             jax.ShapeDtypeStruct(block, BF16),
             jax.ShapeDtypeStruct((ep_count,) + block, BF16),
-            jax.ShapeDtypeStruct((ep_count,) + meta.shape, F32),
+            jax.ShapeDtypeStruct((meta.shape[0], ep_count * seq_count), F32),
         ),
         in_specs=[IN_VMEM] * 4,
         out_specs=(IN_VMEM,) * 4,
@@ -475,13 +615,10 @@
         + tp_sems
         + tp_sems
         + [dma((ep_count,))] * 4,
-        compiler_params=talk(1),
+        compiler_params=talk(1, 12),
         name="resid",
     )(terms, tokens, ffn_gain[None, :], meta)
 
-    first_slot = (lax.axis_index("ep") * (expert_dev * capacity)).astype(F32)
-    flat_meta = jnp.swapaxes(metas, 0, 1).reshape(meta.shape[0], ep_count * seq_count)
-    flat_meta = flat_meta - jnp.where(jnp.arange(meta.shape[0])[:, None] < top_count, first_slot, 0.0)
     whole = lambda shape: pl.BlockSpec(shape, lambda e: (0,) * len(shape))
     parts = pl.pallas_call(
         functools.partial(up_kernel, top=top_count, cap=capacity, seqs=seq_count, width=hidden),
@@ -498,23 +635,34 @@
         name="gate_up",
     )(flat_meta, rows_all.reshape(ep_count * seq_count, slice_width), expert_gate, expert_up)
 
-    inner = pl.pallas_call(
+    pieces = min(8, slot_count // 64)
+    piece = slot_count // (4 * pieces)
+    steps_wide = (2, pieces, piece, 2 * hidden)
+    inner, shared_own = pl.pallas_call(
         functools.partial(inner_kernel, tp_count=tp_count, ep_count=ep_count),
-        out_shape=jax.ShapeDtypeStruct((tp_count, own_slots, hidden), BF16),
-        in_specs=[IN_VMEM],
-        out_specs=IN_VMEM,
-        scratch_shapes=[pltpu.VMEM((chips, own_slots, 2 * hidden), BF16)] * 3
-        + [pltpu.VMEM((tp_count, own_slots, hidden), BF16)]
-        + tp_sems
+        out_shape=(
+            jax.ShapeDtypeStruct((2, 2, pieces, piece, hidden), BF16),
+            jax.ShapeDtypeStruct(block, F32),
+        ),
+        in_specs=[IN_VMEM] * 5,
+        out_specs=(IN_VMEM,) * 2,
+        scratch_shapes=[pltpu.VMEM(steps_wide, BF16)] * 3
+        + [
+            pltpu.VMEM((2, 2, pieces, piece, hidden), BF16),
+            pltpu.VMEM((seq_count, model_width), BF16),
+        ]
+        + [pltpu.VMEM((chips,) + block, BF16)] * 3
+        + [dma((2, pieces))] * 8
         + tp_sems,
-        compiler_params=talk(2),
+        compiler_params=talk(2, 20),
         name="inner",
-    )(parts.reshape(tp_count, own_slots, 2 * hidden))
-
-    shared_gate_rows = jnp.dot(ffn_rows, shared_gate, preferred_element_type=F32)
-    shared_up_rows = jnp.dot(ffn_rows, shared_up, preferred_element_type=F32)
-    shared_inner = (jax.nn.silu(shared_gate_rows) * shared_up_rows).astype(BF16)
-    shared_terms = jnp.dot(shared_inner, shared_down, preferred_element_type=F32).astype(BF16)
+    )(
+        parts.reshape(2, 2, pieces, piece, 2 * hidden),
+        ffn_rows,
+        shared_gate,
+        shared_up,
+        shared_down,
+    )
 
     routed = pl.pallas_call(
         functools.partial(down_kernel, top=top_count, cap=capacity, seqs=seq_count),
@@ -536,13 +684,10 @@
         out_shape=jax.ShapeDtypeStruct(block, BF16),
         in_specs=[IN_VMEM] * 3,
         out_specs=IN_VMEM,
-        scratch_shapes=[pltpu.VMEM((ep_count,) + block, BF16)]
-        + [pltpu.VMEM((chips,) + block, BF16)] * 3
-        + tp_sems
-        + [dma((ep_count,))] * 2,
-        compiler_params=talk(3),
+        scratch_shapes=[pltpu.VMEM((ep_count,) + block, BF16)] + [dma((ep_count,))] * 2,
+        compiler_params=talk(3, 4),
         name="mixed",
-    )(routed.reshape((ep_count,) + block), shared_terms, resid_own)
+    )(routed.reshape((ep_count,) + block), shared_own, resid_own)
     return (mixed, new_real, new_imag)
 
 

time: 117 us -> 102 us (0.87)
  Pallas kernels: 104 us -> 83.2 us
  local copies, waits for them, and re-layouts: 4.54 us -> 17.4 us
  matrix products: 3.97 us -> 0 us
  other arithmetic: 3.53 us -> 0 us
    unnamed x7 -> x47, local copies, waits for them, and re-layouts: 1.49 us -> 17.4 us
    pallas_call x1, Pallas kernels: 15.2 us -> 6.83 us  [local(): pl.pallas_call(functools.partial(mixed_kernel, tp_count=tp_count, ep_coun...]
    dot_general x3 -> x0, matrix products: 3.97 us -> none  [the longest x1 2.42 us: local(): jnp.dot(shared_inner, shared_down, preferred_element_type=F32).astype(BF16)]
    pallas_call x1, Pallas kernels: 6.18 us -> 2.26 us  [local(): pl.pallas_call(functools.partial(up_kernel, top=top_count, cap=capacity,...]
    pallas_call x1, Pallas kernels: 5.58 us -> 2.26 us  [local(): pl.pallas_call(functools.partial(mixer_kernel, groups=groups, experts=exp...]
    pallas_call x1, Pallas kernels: 5.16 us -> 2.33 us  [local(): pl.pallas_call(functools.partial(down_kernel, top=top_count, cap=capacity...]
    pallas_call x1, Pallas kernels: 27.7 us -> 25.7 us  [local(): pl.pallas_call(functools.partial(resid_kernel, tp_count=tp_count, ep_coun...]
where the time goes in v2:
time: 102 us; the launch traced here: 101 us
  Pallas kernels  83.2 us (82%)
  local copies, waits for them, and re-layouts  17.4 us (17%)
    pallas_call x1, Pallas kernels, local(): pl.pallas_call(functools.partial(inner_kernel, tp_count=tp_count, ep_coun...  43.8 us
    pallas_call x1, Pallas kernels, local(): pl.pallas_call(functools.partial(resid_kernel, tp_count=tp_count, ep_coun...  25.7 us
    unnamed x47, local copies, waits for them, and re-layouts  17.4 us
    pallas_call x1, Pallas kernels, local(): pl.pallas_call(functools.partial(mixed_kernel, tp_count=tp_count, ep_coun...  6.83 us
    pallas_call x1, Pallas kernels, local(): pl.pallas_call(functools.partial(down_kernel, top=top_count, cap=capacity...  2.33 us
    pallas_call x1, Pallas kernels, local(): pl.pallas_call(functools.partial(mixer_kernel, groups=groups, experts=exp...  2.26 us
    pallas_call x1, Pallas kernels, local(): pl.pallas_call(functools.partial(up_kernel, top=top_count, cap=capacity,...  2.26 us

profile of v2, /device:TPU:0, one launch (start us, length us, event | category | flops | bytes accessed | tf_op | source)
XLA Modules:
  0.0 101.3 jit_solution(13574542601581154480)
XLA Ops:
  0.6 0.0 copy-start
  0.6 0.0 copy-start.3
  0.7 1.7 %copy-done.3 = bf16[4096,256]{1,0:T(8,128)(2,1)S(1)} copy-done((bf16[4096,256]{1,0:T(8,128)(2,1)S(1)}, bf16[4096,256]{1,0:T(8,128)(2,1)}, u32[]{:S(2)}) %copy-start.3) | copy-done | bytes 2097176
  2.4 0.0 copy-start.4
  2.4 1.7 %copy-done.4 = bf16[256,4096]{1,0:T(8,128)(2,1)S(1)} copy-done((bf16[256,4096]{1,0:T(8,128)(2,1)S(1)}, bf16[256,4096]{1,0:T(8,128)(2,1)}, u32[]{:S(2)}) %copy-start.4) | copy-done | bytes 2097176
  4.1 0.0 copy-start.5
  4.1 1.0 %copy-done.5 = bf16[64,4096]{1,0:T(8,128)(2,1)S(1)} copy-done((bf16[64,4096]{1,0:T(8,128)(2,1)S(1)}, bf16[64,4096]{1,0:T(8,128)(2,1)}, u32[]{:S(2)}) %copy-start.5) | copy-done | bytes 524312
  5.2 0.0 copy-start.9
  5.2 0.9 copy-done.9
  6.1 0.9 copy-done.10
  7.1 0.0 copy-start.11
  7.1 0.8 copy-done.11
  7.9 0.0 copy-start.12
  7.9 0.8 copy-done.12
  8.7 0.0 copy-start.13
  8.7 0.8 copy-done.13
  9.6 0.0 copy-start.14
  9.6 0.8 copy-done.14
  10.4 0.0 copy-start.15
  10.4 0.7 copy-done.15
  11.1 0.0 copy-start.17
  11.1 0.7 copy-done.17
  11.8 0.0 copy-start.18
  11.8 0.7 copy-done.18
  12.5 0.0 copy-start.19
  12.5 0.7 copy-done.19
  13.2 0.0 copy-start.20
  13.2 0.7 copy-done.20
  13.9 0.0 copy-start.21
  13.9 0.7 copy-done.21
  14.6 0.0 copy-start.22
  14.6 0.7 copy-done.22
  15.2 2.3 %mixer.1 = (bf16[64,4096]{1,0:T(8,128)(2,1)S(1)}, f32[64,1024]{1,0:T(8,128)}, f32[64,1024]{1,0:T(8,128)}, f32[8,64]{1,0:T(8,128)S(1)}) custom-call(bf16[64,4096]{1,0:T(8,128)(2,1)S(1)} %copy-done.5, f32[1,4096]{1,0:T(1,128)S(1)} %bitcast.16, bf16[4096,256]{1,0:T(8,128)(2,1)S(1)} %copy-done.3, f32[1,1024]{1,0:T(1,128)S(1)} %bitcast.18, ...), custom_call_target="tpu_custom_call" | custom-call | tf_op jit(solution)/shard_map/mixer/pallas_call | solution.py:564
  17.5 0.0 copy-done.16
  17.5 25.7 %resid.1 = (bf16[64,4096]{1,0:T(8,128)(2,1)S(1)}, bf16[64,512]{1,0:T(8,128)(2,1)S(1)}, bf16[4,64,512]{2,1,0:T(8,128)(2,1)S(1)}, f32[8,256]{1,0:T(8,128)S(1)}) custom-call(bf16[64,4096]{1,0:T(8,128)(2,1)S(1)} %get-tuple-element.13.terms_ref, bf16[64,4096]{1,0:T(8,128)(2,1)S(1)} %copy-done.5, f32[1,4096]{1,0:T(1,128)S(1)} %bitcast.17, ...), custom_call_target="tpu_custom_call" | custom-call | tf_op jit(solution)/shard_map/resid/pallas_call | solution.py:595
  43.1 0.0 copy-done
  43.2 0.0 copy-start.1
  43.2 2.2 %copy-done.1 = bf16[4,512,1024]{2,1,0:T(8,128)(2,1)S(1)} copy-done((bf16[4,512,1024]{2,1,0:T(8,128)(2,1)S(1)}, bf16[4,512,1024]{2,1,0:T(8,128)(2,1)}, u32[]{:S(2)}) %copy-start.1) | copy-done | bytes 4194328
  45.4 2.3 %gate_up.1 = bf16[512,2048]{1,0:T(8,128)(2,1)S(1)} custom-call(f32[8,256]{1,0:T(8,128)S(1)} %get-tuple-element.15.meta_ref, bf16[256,512]{1,0:T(8,128)(2,1)S(1)} %bitcast.15, bf16[4,512,1024]{2,1,0:T(8,128)(2,1)S(1)} %copy-done, bf16[4,512,1024]{2,1,0:T(8,128)(2,1)S(1)} %copy-done.1), custom_call_target="tpu_custom_call" | custom-call | tf_op jit(solution)/shard_map/gate_up/pallas_call | solution.py:623
  47.6 0.0 copy-start.2
  47.6 0.0 copy-done.6
  47.6 0.0 copy-done.7
  47.7 0.0 copy-done.8
  47.7 43.8 %inner.1 = (bf16[2,2,8,16,1024]{4,3,2,1,0:T(8,128)(2,1)S(1)}, f32[64,512]{1,0:T(8,128)S(1)}) custom-call(bf16[2,2,8,16,2048]{4,3,2,1,0:T(8,128)(2,1)S(1)} %bitcast.12, bf16[64,4096]{1,0:T(8,128)(2,1)S(1)} %get-tuple-element.17.ffn_ref, bf16[4096,128]{1,0:T(8,128)(2,1)S(1)} %copy-done.6, bf16[4096,128]{1,0:T(8,128)(2,1)S(1)} %copy-done.7, ...), custom_call_target="tpu_custom_call" | custom-call | tf_op jit(solution)/shard_map/inner/pallas_call | solution.py:641
  91.5 0.0 copy-done.2
  91.5 2.3 %down.1 = bf16[256,512]{1,0:T(8,128)(2,1)S(1)} custom-call(f32[8,256]{1,0:T(8,128)S(1)} %get-tuple-element.15.meta_ref, bf16[512,1024]{1,0:T(8,128)(2,1)S(1)} %bitcast.13, bf16[4,1024,512]{2,1,0:T(8,128)(2,1)S(1)} %copy-done.2), custom_call_target="tpu_custom_call" | custom-call | tf_op jit(solution)/shard_map/down/pallas_call | solution.py:667
  93.8 6.8 %mixed.1 = bf16[64,512]{1,0:T(8,128)(2,1)S(1)} custom-call(bf16[4,64,512]{2,1,0:T(8,128)(2,1)S(1)} %bitcast.14, f32[64,512]{1,0:T(8,128)S(1)} %get-tuple-element.19.shared_ref, bf16[64,512]{1,0:T(8,128)(2,1)S(1)} %get-tuple-element.20.resid_ref), custom_call_target="tpu_custom_call" | custom-call | tf_op jit(solution)/shard_map/mixed/pallas_call | solution.py:682
  100.7 0.6 copy.27
  (5 shorter events, 0.0 us)
Async XLA Ops:
  0.6 42.5 %copy-start = (bf16[4,512,1024]{2,1,0:T(8,128)(2,1)S(1)}, bf16[4,512,1024]{2,1,0:T(8,128)(2,1)}, u32[]{:S(2)}) copy-start(bf16[4,512,1024]{2,1,0:T(8,128)(2,1)} %gate_ref.1) | copy-start | bytes 12582916
  0.6 1.7 %copy-start.3 = (bf16[4096,256]{1,0:T(8,128)(2,1)S(1)}, bf16[4096,256]{1,0:T(8,128)(2,1)}, u32[]{:S(2)}) copy-start(bf16[4096,256]{1,0:T(8,128)(2,1)} %w_in_ref.1) | copy-start | bytes 6291460
  2.4 1.7 %copy-start.4 = (bf16[256,4096]{1,0:T(8,128)(2,1)S(1)}, bf16[256,4096]{1,0:T(8,128)(2,1)}, u32[]{:S(2)}) copy-start(bf16[256,4096]{1,0:T(8,128)(2,1)} %w_out_ref.1) | copy-start | bytes 6291460
  4.1 1.0 %copy-start.5 = (bf16[64,4096]{1,0:T(8,128)(2,1)S(1)}, bf16[64,4096]{1,0:T(8,128)(2,1)}, u32[]{:S(2)}) copy-start(bf16[64,4096]{1,0:T(8,128)(2,1)} %tokens_ref.3) | copy-start | bytes 1572868
  5.2 0.9 copy-start.9
  6.1 0.9 copy-start.10
  7.1 0.8 copy-start.11
  7.9 0.8 copy-start.12
  8.7 0.8 copy-start.13
  9.6 0.8 copy-start.14
  10.4 0.7 copy-start.15
  11.1 0.7 copy-start.17
  11.8 0.7 copy-start.18
  12.5 0.7 copy-start.19
  13.2 0.7 copy-start.20
  13.9 0.7 copy-start.21
  14.6 0.7 copy-start.22
  15.2 2.3 %copy-start.16 = (f32[4096]{0:T(1024)S(1)}, f32[4096]{0:T(1024)}, u32[]{:S(2)}) copy-start(f32[4096]{0:T(1024)} %param.25) | copy-start | bytes 49156
  43.2 2.2 %copy-start.1 = (bf16[4,512,1024]{2,1,0:T(8,128)(2,1)S(1)}, bf16[4,512,1024]{2,1,0:T(8,128)(2,1)}, u32[]{:S(2)}) copy-start(bf16[4,512,1024]{2,1,0:T(8,128)(2,1)} %up_ref.1) | copy-start | bytes 12582916
  45.3 2.3 %copy-start.6 = (bf16[4096,128]{1,0:T(8,128)(2,1)S(1)}, bf16[4096,128]{1,0:T(8,128)(2,1)}, u32[]{:S(2)}) copy-start(bf16[4096,128]{1,0:T(8,128)(2,1)} %shared_gate_ref.1) | copy-start | bytes 3145732
  45.3 2.3 %copy-start.7 = (bf16[4096,128]{1,0:T(8,128)(2,1)S(1)}, bf16[4096,128]{1,0:T(8,128)(2,1)}, u32[]{:S(2)}) copy-start(bf16[4096,128]{1,0:T(8,128)(2,1)} %shared_up_ref.1) | copy-start | bytes 3145732
  45.4 2.3 %copy-start.8 = (bf16[128,4096]{1,0:T(8,128)(2,1)S(1)}, bf16[128,4096]{1,0:T(8,128)(2,1)}, u32[]{:S(2)}) copy-start(bf16[128,4096]{1,0:T(8,128)(2,1)} %shared_down_ref.1) | copy-start | bytes 3145732
  47.6 43.9 %copy-start.2 = (bf16[4,1024,512]{2,1,0:T(8,128)(2,1)S(1)}, bf16[4,1024,512]{2,1,0:T(8,128)(2,1)}, u32[]{:S(2)}) copy-start(bf16[4,1024,512]{2,1,0:T(8,128)(2,1)} %down_ref.1) | copy-start | bytes 12582916

commit v3 on v2

--- a/solution.py
+++ b/solution.py
@@ -423,7 +423,7 @@
 
         to_partner(h, k).start()
 
-    gap = 2
+    gap, gap_back = 3, 2
 
     def one_step(i):
         for h in range(2):
@@ -434,7 +434,7 @@
                 sum_step(h, k)
 
         for h in range(2):
-            late = i - gap * (chips - 1) - gap * (chips - 1 - stage[h])
+            late = i - gap * (chips - 1) - gap_back * (chips - 1 - stage[h])
 
             @pl.when((stage[h] < chips - 1) & (late >= 0) & (late < pieces))
             def _():
@@ -450,7 +450,7 @@
         for h in range(2):
             to_mate(h, k).start()
 
-    total_steps = pieces + 2 * gap * (chips - 1)
+    total_steps = pieces + (gap + gap_back) * (chips - 1)
     steps(0, 3)
     rows = ffn_ref[...]
     gate = jnp.dot(rows, shared_gate_ref[...], preferred_element_type=F32)
@@ -571,7 +571,7 @@
         ),
         in_specs=[IN_VMEM] * 16,
         out_specs=(IN_VMEM,) * 4,
-        compiler_params=local_params,
+        compiler_params=pltpu.CompilerParams(vmem_limit_bytes=3 * VMEM_LIMIT),
         name="mixer",
     )(
         tokens,

time: 102 us -> 93.3 us (0.915)
  local copies, waits for them, and re-layouts: 17.4 us -> 6.75 us
  Pallas kernels: 83.2 us -> 85.5 us
    unnamed x47 -> x21, local copies, waits for them, and re-layouts: 17.4 us -> 6.75 us
    pallas_call x1, Pallas kernels: 2.26 us -> 5.51 us  [local(): pl.pallas_call(functools.partial(mixer_kernel, groups=groups, experts=exp...]
    pallas_call x1, Pallas kernels: 43.8 us -> 42.3 us  [local(): pl.pallas_call(functools.partial(inner_kernel, tp_count=tp_count, ep_coun...]
where the time goes in v3:
time: 93.3 us; the launch traced here: 93 us
  Pallas kernels  85.5 us (92%)
  local copies, waits for them, and re-layouts  6.75 us (7%)
    pallas_call x1, Pallas kernels, local(): pl.pallas_call(functools.partial(inner_kernel, tp_count=tp_count, ep_coun...  42.3 us
    pallas_call x1, Pallas kernels, local(): pl.pallas_call(functools.partial(resid_kernel, tp_count=tp_count, ep_coun...  25.7 us
    pallas_call x1, Pallas kernels, local(): pl.pallas_call(functools.partial(mixed_kernel, tp_count=tp_count, ep_coun...  7.45 us
    unnamed x21, local copies, waits for them, and re-layouts  6.75 us
    pallas_call x1, Pallas kernels, local(): pl.pallas_call(functools.partial(mixer_kernel, groups=groups, experts=exp...  5.51 us
    pallas_call x1, Pallas kernels, local(): pl.pallas_call(functools.partial(down_kernel, top=top_count, cap=capacity...  2.33 us
    pallas_call x1, Pallas kernels, local(): pl.pallas_call(functools.partial(up_kernel, top=top_count, cap=capacity,...  2.27 us

profile of v3, /device:TPU:0, one launch (start us, length us, event | category | flops | bytes accessed | tf_op | source)
XLA Modules:
  0.0 93.0 jit_solution(7550613555993596348)
XLA Ops:
  0.6 0.0 copy-start.3
  0.6 0.0 copy-start.8
  0.7 5.5 %mixer.1 = (bf16[64,4096]{1,0:T(8,128)(2,1)}, f32[64,1024]{1,0:T(8,128)}, f32[64,1024]{1,0:T(8,128)}, f32[8,64]{1,0:T(8,128)}) custom-call(bf16[64,4096]{1,0:T(8,128)(2,1)} %tokens_ref.3, f32[1,4096]{1,0:T(1,128)} %bitcast.17, bf16[4096,256]{1,0:T(8,128)(2,1)} %w_in_ref.1, f32[1,1024]{1,0:T(1,128)} %bitcast.18, f32[1,1024]{1,0:T(1,128)} %bitcast.19, ...), custom_call_target="tpu_custom_call" | custom-call | tf_op jit(solution)/shard_map/mixer/pallas_call | solution.py:564
  6.2 0.0 copy-done.3
  6.2 0.0 copy-done.8
  6.2 0.0 copy-start.7
  6.2 1.0 %copy-done.7 = bf16[64,4096]{1,0:T(8,128)(2,1)S(1)} copy-done((bf16[64,4096]{1,0:T(8,128)(2,1)S(1)}, bf16[64,4096]{1,0:T(8,128)(2,1)}, u32[]{:S(2)}) %copy-start.7) | copy-done | bytes 524312
  7.2 0.0 copy-start.9
  7.2 0.7 copy-done.9
  7.9 25.7 %resid.1 = (bf16[64,4096]{1,0:T(8,128)(2,1)S(1)}, bf16[64,512]{1,0:T(8,128)(2,1)S(1)}, bf16[4,64,512]{2,1,0:T(8,128)(2,1)S(1)}, f32[8,256]{1,0:T(8,128)S(1)}) custom-call(bf16[64,4096]{1,0:T(8,128)(2,1)S(1)} %copy-done.7, bf16[64,4096]{1,0:T(8,128)(2,1)S(1)} %copy-done.3, f32[1,4096]{1,0:T(1,128)S(1)} %bitcast.16, f32[8,64]{1,0:T(8,128)S(1)} %copy-done.9), custom_call_target="tpu_custom_call" | custom-call | tf_op jit(solution)/shard_map/resid/pallas_call | solution.py:595
  33.6 0.0 copy-start
  33.6 2.2 %copy-done = bf16[4,512,1024]{2,1,0:T(8,128)(2,1)S(1)} copy-done((bf16[4,512,1024]{2,1,0:T(8,128)(2,1)S(1)}, bf16[4,512,1024]{2,1,0:T(8,128)(2,1)}, u32[]{:S(2)}) %copy-start) | copy-done | bytes 4194328
  35.8 0.0 copy-start.1
  35.8 2.2 %copy-done.1 = bf16[4,512,1024]{2,1,0:T(8,128)(2,1)S(1)} copy-done((bf16[4,512,1024]{2,1,0:T(8,128)(2,1)S(1)}, bf16[4,512,1024]{2,1,0:T(8,128)(2,1)}, u32[]{:S(2)}) %copy-start.1) | copy-done | bytes 4194328
  38.0 0.0 copy-start.4
  38.0 0.0 copy-start.5
  38.0 0.0 copy-start.6
  38.0 2.3 %gate_up.1 = bf16[512,2048]{1,0:T(8,128)(2,1)S(1)} custom-call(f32[8,256]{1,0:T(8,128)S(1)} %get-tuple-element.15.meta_ref, bf16[256,512]{1,0:T(8,128)(2,1)S(1)} %bitcast.15, bf16[4,512,1024]{2,1,0:T(8,128)(2,1)S(1)} %copy-done, bf16[4,512,1024]{2,1,0:T(8,128)(2,1)S(1)} %copy-done.1), custom_call_target="tpu_custom_call" | custom-call | tf_op jit(solution)/shard_map/gate_up/pallas_call | solution.py:623
  40.2 0.0 copy-start.2
  40.2 0.0 copy-done.4
  40.3 0.0 copy-done.5
  40.3 0.0 copy-done.6
  40.3 42.3 %inner.1 = (bf16[2,2,8,16,1024]{4,3,2,1,0:T(8,128)(2,1)S(1)}, f32[64,512]{1,0:T(8,128)S(1)}) custom-call(bf16[2,2,8,16,2048]{4,3,2,1,0:T(8,128)(2,1)S(1)} %bitcast.12, bf16[64,4096]{1,0:T(8,128)(2,1)S(1)} %get-tuple-element.17.ffn_ref, bf16[4096,128]{1,0:T(8,128)(2,1)S(1)} %copy-done.4, bf16[4096,128]{1,0:T(8,128)(2,1)S(1)} %copy-done.5, ...), custom_call_target="tpu_custom_call" | custom-call | tf_op jit(solution)/shard_map/inner/pallas_call | solution.py:641
  82.6 0.0 copy-done.2
  82.6 2.3 %down.1 = bf16[256,512]{1,0:T(8,128)(2,1)S(1)} custom-call(f32[8,256]{1,0:T(8,128)S(1)} %get-tuple-element.15.meta_ref, bf16[512,1024]{1,0:T(8,128)(2,1)S(1)} %bitcast.13, bf16[4,1024,512]{2,1,0:T(8,128)(2,1)S(1)} %copy-done.2), custom_call_target="tpu_custom_call" | custom-call | tf_op jit(solution)/shard_map/down/pallas_call | solution.py:667
  84.9 7.5 %mixed.1 = bf16[64,512]{1,0:T(8,128)(2,1)S(1)} custom-call(bf16[4,64,512]{2,1,0:T(8,128)(2,1)S(1)} %bitcast.14, f32[64,512]{1,0:T(8,128)S(1)} %get-tuple-element.19.shared_ref, bf16[64,512]{1,0:T(8,128)(2,1)S(1)} %get-tuple-element.20.resid_ref), custom_call_target="tpu_custom_call" | custom-call | tf_op jit(solution)/shard_map/mixed/pallas_call | solution.py:682
  92.4 0.6 copy.27
Async XLA Ops:
  0.6 5.5 %copy-start.3 = (bf16[64,4096]{1,0:T(8,128)(2,1)S(1)}, bf16[64,4096]{1,0:T(8,128)(2,1)}, u32[]{:S(2)}) copy-start(bf16[64,4096]{1,0:T(8,128)(2,1)} %tokens_ref.3) | copy-start | bytes 1572868
  0.6 5.5 %copy-start.8 = (f32[4096]{0:T(1024)S(1)}, f32[4096]{0:T(1024)}, u32[]{:S(2)}) copy-start(f32[4096]{0:T(1024)} %param.25) | copy-start | bytes 49156
  6.2 1.0 %copy-start.7 = (bf16[64,4096]{1,0:T(8,128)(2,1)S(1)}, bf16[64,4096]{1,0:T(8,128)(2,1)}, u32[]{:S(2)}) copy-start(bf16[64,4096]{1,0:T(8,128)(2,1)} %get-tuple-element.13.terms_ref) | copy-start | bytes 1572868
  7.2 0.7 copy-start.9
  33.6 2.2 %copy-start = (bf16[4,512,1024]{2,1,0:T(8,128)(2,1)S(1)}, bf16[4,512,1024]{2,1,0:T(8,128)(2,1)}, u32[]{:S(2)}) copy-start(bf16[4,512,1024]{2,1,0:T(8,128)(2,1)} %gate_ref.1) | copy-start | bytes 12582916
  35.8 2.2 %copy-start.1 = (bf16[4,512,1024]{2,1,0:T(8,128)(2,1)S(1)}, bf16[4,512,1024]{2,1,0:T(8,128)(2,1)}, u32[]{:S(2)}) copy-start(bf16[4,512,1024]{2,1,0:T(8,128)(2,1)} %up_ref.1) | copy-start | bytes 12582916
  38.0 2.3 %copy-start.4 = (bf16[4096,128]{1,0:T(8,128)(2,1)S(1)}, bf16[4096,128]{1,0:T(8,128)(2,1)}, u32[]{:S(2)}) copy-start(bf16[4096,128]{1,0:T(8,128)(2,1)} %shared_gate_ref.1) | copy-start | bytes 3145732
  38.0 2.3 %copy-start.5 = (bf16[4096,128]{1,0:T(8,128)(2,1)S(1)}, bf16[4096,128]{1,0:T(8,128)(2,1)}, u32[]{:S(2)}) copy-start(bf16[4096,128]{1,0:T(8,128)(2,1)} %shared_up_ref.1) | copy-start | bytes 3145732
  38.0 2.3 %copy-start.6 = (bf16[128,4096]{1,0:T(8,128)(2,1)S(1)}, bf16[128,4096]{1,0:T(8,128)(2,1)}, u32[]{:S(2)}) copy-start(bf16[128,4096]{1,0:T(8,128)(2,1)} %shared_down_ref.1) | copy-start | bytes 3145732
  40.2 42.4 %copy-start.2 = (bf16[4,1024,512]{2,1,0:T(8,128)(2,1)S(1)}, bf16[4,1024,512]{2,1,0:T(8,128)(2,1)}, u32[]{:S(2)}) copy-start(bf16[4,1024,512]{2,1,0:T(8,128)(2,1)} %down_ref.1) | copy-start | bytes 12582916
